TPU v7x, 256 devices: a whole 4x4x8 slice. The times are simulated.
256 devices in a mesh: sp: 32 (over z, x), tp: 8 (over y, core).
Axes of the slice: x: 4, y: 4, z: 8, core: 2. Of those that a mesh axis runs over, the one named last changes fastest.
Arguments:
- query_rows: bfloat16 [32768, 1024], P('sp', 'tp'), may hold values from -8 to 8
- key_rows: bfloat16 [32768, 1024], P('sp', 'tp'), may hold values from -8 to 8
- value_rows: bfloat16 [32768, 1024], P('sp', 'tp'), may hold values from -6 to 6
- forget_cum: float32 [16, 32768], P('tp', 'sp'), may hold values from -32768 to 0, as said below
- doc_ids: int32 [32768], P('sp'), may hold values from 0 to 15, never falling along the last dimension, each value on 1 to 3072 neighbouring positions
- residual: bfloat16 [32768, 2048], P(('sp', 'tp')), may hold values from -6 to 6
- out_weight: bfloat16 [1024, 2048], replicated, may hold values from -1.5 to 1.5
- norm_gain: float32 [2048], replicated, may hold values from 0.1 to 1.9
- expert_ids: int32 [32768, 2], P(('sp', 'tp')), may hold values from 0 to 31, as said below
- route_weights: float32 [32768, 2], P(('sp', 'tp')), may hold values from 0.2 to 1
- gate_proj: bfloat16 [32, 2048, 512], P('sp'), may hold values from -0.125 to 0.125
- up_proj: bfloat16 [32, 2048, 512], P('sp'), may hold values from -0.125 to 0.125
- down_proj: bfloat16 [32, 512, 2048], P('sp'), may hold values from -0.25 to 0.25
Outputs:
- layer_out: bfloat16 [32768, 2048], P(('sp', 'tp'))
Inputs may be any that keep to these rules, and one draw needn't show every extreme that they name: `forget_cum`: each head's values never rise along the positions. `doc_ids`: document numbers never fall along the positions; a document holds at most 3072 positions, and one holds exactly 3072. `expert_ids`: a token's 2 experts differ and lie in one group of 4 consecutive experts; among the 128 rows of one device no expert is named more than 20 times, and in every draw one expert is named exactly 20 times by the rows of every device.
All inputs are finite; a program needn't handle non-finite values.
Results may differ from a plain program's by a relative error of at most 0.0054.
Values may be sent and summed in bfloat16 or wider, within the bound.
A program may use at most 128 MiB of HBM per device.

v0:
```python
import jax
import jax.numpy as jnp
from jax import lax
from jax.sharding import PartitionSpec as P

EPG = 4
TOPK = 2
REACH = 3


norm_eps = 1e-06


def from_behind(block, axis, distance):
    devices = range(lax.axis_size(axis))
    route = [(i - distance, i) for i in devices if i - distance in devices]
    return lax.ppermute(block, axis, route)


def join_blocks(key_blocks, mark_blocks):
    stacked = jnp.concatenate(key_blocks, axis=1)
    gates = jnp.concatenate([piece[0] for piece in mark_blocks], axis=1)
    documents = jnp.concatenate([piece[1] for piece in mark_blocks], axis=0)
    return (stacked, gates, documents)


def per_device(
    query_rows,
    key_rows,
    value_rows,
    forget_cum,
    doc_ids,
    residual,
    out_weight,
    norm_gain,
    expert_ids,
    route_weights,
    gate_proj,
    up_proj,
    down_proj,
):
    tok_dev = query_rows.shape[0]
    width_dev = query_rows.shape[1]
    heads_dev = forget_cum.shape[0]
    head_size = width_dev // heads_dev
    first_position = lax.axis_index("sp") * tok_dev
    own_keys = jnp.stack([key_rows, value_rows])
    own_marks = (forget_cum, doc_ids)
    joined_keys = own_keys
    joined_marks = own_marks
    covered = 1
    while covered < REACH + 1:
        moved_keys = from_behind(joined_keys, "sp", covered)
        moved_marks = from_behind((joined_marks[0], joined_marks[1]), "sp", covered)
        stacked_now, gates_now, docs_now = join_blocks(
            [moved_keys, joined_keys], [moved_marks, joined_marks]
        )
        joined_keys = stacked_now
        joined_marks = (gates_now, docs_now)
        covered = covered * 2
    joined = (joined_keys, joined_marks[0], joined_marks[1])
    stacked, gates_all, docs_all = joined
    span = stacked.shape[1]
    key_split = stacked[0].reshape(span, heads_dev, head_size)
    value_split = stacked[1].reshape(span, heads_dev, head_size)
    key_positions = first_position - (span - tok_dev) + jnp.arange(span, dtype=jnp.int32)
    block_rows = min(512, tok_dev)
    scale = head_size ** (-0.5)

    def attend(index):
        query_start = index * block_rows
        query = lax.dynamic_slice_in_dim(query_rows, query_start, block_rows, 0).reshape(
            block_rows, heads_dev, head_size
        )
        query_gate = lax.dynamic_slice_in_dim(forget_cum, query_start, block_rows, 1)
        query_doc = lax.dynamic_slice_in_dim(doc_ids, query_start, block_rows, 0)
        query_pos = first_position + query_start + jnp.arange(block_rows, dtype=jnp.int32)
        pieces = []
        seen = []
        for place in range(REACH + 1):
            lower = place * tok_dev
            key_doc = docs_all[lower : lower + tok_dev]
            key_pos = key_positions[lower : lower + tok_dev]
            visible = (
                (key_doc[-1] >= query_doc[0]) & (key_pos[0] <= query_pos[-1]) & (key_pos[-1] >= 0)
            )

            def compute(lower=lower, key_doc=key_doc, key_pos=key_pos):
                score = (
                    jnp.einsum(
                        "qhd,khd->hqk",
                        query,
                        key_split[lower : lower + tok_dev],
                        preferred_element_type=jnp.float32,
                    )
                    * scale
                )
                score = score + query_gate[:, :, None] - gates_all[:, None, lower : lower + tok_dev]
                allowed = (key_pos[None, :] <= query_pos[:, None]) & (
                    key_doc[None, :] == query_doc[:, None]
                )
                return jnp.where(allowed[None], score, -jnp.inf)

            def blank():
                return jnp.full((heads_dev, block_rows, tok_dev), -jnp.inf, jnp.float32)

            pieces.append(lax.cond(visible, compute, blank))
            seen.append(visible)
        top = pieces[0].max(axis=-1)
        for piece in pieces[1:]:
            top = jnp.maximum(top, piece.max(axis=-1))
        total = jnp.zeros((heads_dev, block_rows), jnp.float32)
        summed = jnp.zeros((block_rows, heads_dev, head_size), jnp.float32)
        for place in range(REACH + 1):
            lower = place * tok_dev

            def weigh(piece=pieces[place], lower=lower):
                expo = jnp.exp(piece - top[..., None])
                rounded = expo.astype(jnp.bfloat16)
                product = jnp.einsum(
                    "hqk,khd->qhd",
                    rounded,
                    value_split[lower : lower + tok_dev],
                    preferred_element_type=jnp.float32,
                )
                return (jnp.sum(expo, axis=-1), product)

            def nothing():
                return (
                    jnp.zeros((heads_dev, block_rows), jnp.float32),
                    jnp.zeros((block_rows, heads_dev, head_size), jnp.float32),
                )

            part_total, part_sum = lax.cond(seen[place], weigh, nothing)
            total = total + part_total
            summed = summed + part_sum
        result = summed / jnp.transpose(total)[:, :, None]
        return result.astype(jnp.bfloat16).reshape(block_rows, width_dev)

    attended = lax.map(attend, jnp.arange(tok_dev // block_rows, dtype=jnp.int32)).reshape(
        tok_dev, width_dev
    )
    tok_loc = residual.shape[0]
    token_heads = lax.all_to_all(attended, "tp", split_axis=0, concat_axis=1, tiled=True)
    mixed = jnp.dot(token_heads, out_weight, preferred_element_type=jnp.float32)
    hidden = residual.astype(jnp.float32) + mixed
    normed = (
        hidden * lax.rsqrt(jnp.mean(hidden * hidden, axis=-1, keepdims=True) + norm_eps) * norm_gain
    ).astype(jnp.bfloat16)
    experts = lax.axis_size("sp")
    groups = experts // EPG
    capacity = max(2, 5 * tok_loc // (4 * groups))
    width = normed.shape[1]
    flat = expert_ids.reshape(-1)
    onehot = (flat[:, None] == jnp.arange(experts, dtype=jnp.int32)[None, :]).astype(jnp.int32)
    earlier = jnp.cumsum(onehot, axis=0) - onehot
    slot_rank = jnp.sum(earlier * onehot, axis=1)
    slot = flat * capacity + slot_rank
    select = (jnp.arange(experts * capacity, dtype=jnp.int32)[:, None] == slot[None, :]).astype(
        jnp.bfloat16
    )
    select_tokens = select.reshape(experts * capacity, tok_loc, TOPK).sum(axis=-1)
    sent = jnp.dot(select_tokens, normed, preferred_element_type=jnp.float32).astype(jnp.bfloat16)
    sent = sent.reshape(experts, capacity, width)
    arrived = lax.all_to_all(sent, "sp", split_axis=0, concat_axis=0, tiled=True)
    rows = arrived.reshape(-1, width)
    gate = jnp.dot(rows, gate_proj[0], preferred_element_type=jnp.float32)
    up = jnp.dot(rows, up_proj[0], preferred_element_type=jnp.float32)
    act = (jax.nn.silu(gate) * up).astype(jnp.bfloat16)
    outcome = jnp.dot(act, down_proj[0], preferred_element_type=jnp.float32).astype(jnp.bfloat16)
    back = lax.all_to_all(
        outcome.reshape(arrived.shape), "sp", split_axis=0, concat_axis=0, tiled=True
    )
    back_rows = back.reshape(experts * capacity, width)
    picked = lax.dot_general(
        select, back_rows, (((0,), (0,)), ((), ())), preferred_element_type=jnp.float32
    )
    picked = picked.reshape(tok_loc, TOPK, width)
    combined = jnp.sum(picked * route_weights[:, :, None], axis=1)
    return (hidden + combined).astype(jnp.bfloat16)


def solution(mesh):
    placed = (
        P("sp", "tp"),
        P("sp", "tp"),
        P("sp", "tp"),
        P("tp", "sp"),
        P("sp"),
        P(("sp", "tp"), None),
        P(),
        P(),
        P(("sp", "tp"), None),
        P(("sp", "tp"), None),
        P("sp", None, None),
        P("sp", None, None),
        P("sp", None, None),
    )
    return jax.shard_map(
        per_device, mesh=mesh, in_specs=placed, out_specs=P(("sp", "tp"), None), check_vma=False
    )
```

profile of v0, /device:TPU:2, one launch (start us, length us, event | category | flops | bytes accessed | tf_op | source)
XLA Modules:
  0.0 412.6 jit_solution(14677040129986016052)
XLA Ops:
  4.6 12.2 %collective-permute-done.2 = bf16[2,1024,128]{2,1,0:T(8,128)(2,1)S(1)} collective-permute-done((bf16[2,1024,128]{2,1,0:T(8,128)(2,1)S(1)}, bf16[2,1024,128]{2,1,0:T(8,128)(2,1)S(1)}, u32[]{:S(2)}, u32[]{:S(2)}) %collective-permute-start.2) | collective-permute-done | bytes 524320 | tf_op jit(solution)/shard_map/ppermute | solution.py:17
  18.9 5.1 %collective-permute-start.3 = (bf16[2,2048,128]{2,1,0:T(8,128)(2,1)}, bf16[2,2048,128]{2,1,0:T(8,128)(2,1)}, u32[]{:S(2)}, u32[]{:S(2)}) collective-permute-start(bf16[2,2048,128]{2,1,0:T(8,128)(2,1)} %maximum_maximum_fusion.2), channel_id=1, source_target_pairs={{0,16},{8,24},{16,32},{24,40},{32,48},{40,56},{48,64},{56,72},{64,... | collective-permute-start | bytes 3145736 | tf_op jit(solution)/shard_map/ppermute | solution.py:17
  36.2 10.7 %collective-permute-done = s32[1024]{0:T(1024)} collective-permute-done((s32[1024]{0:T(1024)}, s32[1024]{0:T(1024)}, u32[]{:S(2)}, u32[]{:S(2)}) %collective-permute-start) | collective-permute-done | bytes 4128 | tf_op jit(solution)/shard_map/ppermute | solution.py:17
  51.6 6.1 %collective-permute-start.5 = (f32[2,2048]{1,0:T(2,128)S(1)}, f32[2,2048]{1,0:T(2,128)}, u32[]{:S(2)}, u32[]{:S(2)}) collective-permute-start(f32[2,2048]{1,0:T(2,128)S(1)} %pad_maximum_fusion.1), channel_id=1, source_target_pairs={{0,16},{8,24},{16,32},{24,40},{32,48},{40,56},{48,64},{56,72},{64,... | collective-permute-start | bytes 49160 | tf_op jit(solution)/shard_map/ppermute | solution.py:17
  63.7 102.0 %while.11 = (s32[]{:T(128)}, bf16[2,512,128]{2,1,0:T(8,128)(2,1)}, s32[2048]{0:T(1024)}, s32[2]{0:T(128)}, s32[1024]{0:T(1024)}, /*index=5*/s32[4096]{0:T(1024)S...) while((s32[]{:T(128)}, bf16[2,512,128]{2,1,0:T(8,128)(2,1)}, ...), condition=%wide.region_25.26_spmd, body=%wide.region_0.25_spmd.sunk | while | flops 1118108160 | bytes 62828020 | solution.py:140
  84.4 5.4 %conditional.17 = (f32[2,512,1024]{2,1,0:T(8,128)}, f32[2,512]{1,0:T(2,128)S(1)}) conditional(s32[]{:T(128)} %convert_element_type.114, () %tuple.133, (s32[4096]{0:T(1024)S(1)}, s32[512]{0:T(512)S(1)}, s32[1024]{0:T(1024)}, s32[512]{0:T(512)S(1)}, bf16[4096,2,64]{0,2,1:T(8,128)(2,1)}, /*index=5*/bf16[512,2,64]{0,2,1:T(8,128)(2,1)S(1)}, ...), branch_computations={%region_7.7_spmd, %region_8.9_spmd} | conditional | flops 141032448 | bytes 5672976 | solution.py:107
  93.6 5.4 %conditional.16 = (f32[2,512,1024]{2,1,0:T(8,128)}, f32[2,512]{1,0:T(2,128)S(1)}) conditional(s32[]{:T(128)} %convert_element_type.113, () %tuple.131, (s32[4096]{0:T(1024)S(1)}, s32[512]{0:T(512)S(1)}, s32[1024]{0:T(1024)}, s32[512]{0:T(512)S(1)}, bf16[4096,2,64]{0,2,1:T(8,128)(2,1)}, /*index=5*/bf16[512,2,64]{0,2,1:T(8,128)(2,1)S(1)}, ...), branch_computations={%region_10.10_spmd, %region_11.12_spmd} | conditional | flops 141032448 | bytes 5672976 | solution.py:107
  99.9 6.1 %conditional.21 = (f32[2,512]{1,0:T(2,128)S(1)}, f32[512,2,64]{0,2,1:T(8,128)S(1)}) conditional(s32[]{:T(128)} %convert_element_type.114, () %tuple.139, (f32[2,512]{1,0:T(2,128)S(1)}, f32[2,512,1024]{2,1,0:T(8,128)}, bf16[4096,2,64]{0,2,1:T(8,128)(2,1)S(1)}) %tuple.140), branch_computations={%region_19.19_spmd, %region_20.21_spmd} | conditional | flops 138411008 | bytes 8925200 | solution.py:134
  106.7 6.1 %conditional.20 = (f32[2,512]{1,0:T(2,128)S(1)}, f32[512,2,64]{0,2,1:T(8,128)S(1)}) conditional(s32[]{:T(128)} %convert_element_type.113, () %tuple.130, (f32[2,512]{1,0:T(2,128)S(1)}, f32[2,512,1024]{2,1,0:T(8,128)}, bf16[4096,2,64]{0,2,1:T(8,128)(2,1)S(1)}) %tuple.138), branch_computations={%region_22.22_spmd, %region_23.24_spmd} | conditional | flops 138411008 | bytes 8925200 | solution.py:134
  135.4 5.4 %conditional.17 = (f32[2,512,1024]{2,1,0:T(8,128)}, f32[2,512]{1,0:T(2,128)S(1)}) conditional(s32[]{:T(128)} %convert_element_type.114, () %tuple.133, (s32[4096]{0:T(1024)S(1)}, s32[512]{0:T(512)S(1)}, s32[1024]{0:T(1024)}, s32[512]{0:T(512)S(1)}, bf16[4096,2,64]{0,2,1:T(8,128)(2,1)}, /*index=5*/bf16[512,2,64]{0,2,1:T(8,128)(2,1)S(1)}, ...), branch_computations={%region_7.7_spmd, %region_8.9_spmd} | conditional | flops 141032448 | bytes 5672976 | solution.py:107
  144.6 5.4 %conditional.16 = (f32[2,512,1024]{2,1,0:T(8,128)}, f32[2,512]{1,0:T(2,128)S(1)}) conditional(s32[]{:T(128)} %convert_element_type.113, () %tuple.131, (s32[4096]{0:T(1024)S(1)}, s32[512]{0:T(512)S(1)}, s32[1024]{0:T(1024)}, s32[512]{0:T(512)S(1)}, bf16[4096,2,64]{0,2,1:T(8,128)(2,1)}, /*index=5*/bf16[512,2,64]{0,2,1:T(8,128)(2,1)S(1)}, ...), branch_computations={%region_10.10_spmd, %region_11.12_spmd} | conditional | flops 141032448 | bytes 5672976 | solution.py:107
  150.9 6.1 %conditional.21 = (f32[2,512]{1,0:T(2,128)S(1)}, f32[512,2,64]{0,2,1:T(8,128)S(1)}) conditional(s32[]{:T(128)} %convert_element_type.114, () %tuple.139, (f32[2,512]{1,0:T(2,128)S(1)}, f32[2,512,1024]{2,1,0:T(8,128)}, bf16[4096,2,64]{0,2,1:T(8,128)(2,1)S(1)}) %tuple.140), branch_computations={%region_19.19_spmd, %region_20.21_spmd} | conditional | flops 138411008 | bytes 8925200 | solution.py:134
  157.7 6.1 %conditional.20 = (f32[2,512]{1,0:T(2,128)S(1)}, f32[512,2,64]{0,2,1:T(8,128)S(1)}) conditional(s32[]{:T(128)} %convert_element_type.113, () %tuple.130, (f32[2,512]{1,0:T(2,128)S(1)}, f32[2,512,1024]{2,1,0:T(8,128)}, bf16[4096,2,64]{0,2,1:T(8,128)(2,1)S(1)}) %tuple.138), branch_computations={%region_22.22_spmd, %region_23.24_spmd} | conditional | flops 138411008 | bytes 8925200 | solution.py:134
  165.7 4.6 %all-to-all-start = ((bf16[8,128,128]{2,1,0:T(8,128)(2,1)}), bf16[8,128,128]{2,1,0:T(8,128)(2,1)S(1)}, u32[]{:S(2)}, u32[]{:S(2)}) async-start(bf16[8,128,128]{2,1,0:T(8,128)(2,1)} %bitcast.103), calls=%async_computation | async-start | bytes 524288 | tf_op jit(solution)/shard_map/all_to_all | solution.py:144
  171.7 6.1 %all-to-all-done = bf16[8,128,128]{2,1,0:T(8,128)(2,1)S(1)} async-done(((bf16[8,128,128]{2,1,0:T(8,128)(2,1)}), bf16[8,128,128]{2,1,0:T(8,128)(2,1)S(1)}, u32[]{:S(2)}, u32[]{:S(2)}) %all-to-all-start) | async-done | bytes 262176 | tf_op jit(solution)/shard_map/all_to_all | solution.py:144
  183.7 5.2 %reshape.354 = bf16[32,20,2048]{2,1,0:T(8,128)(2,1)} reshape(bf16[640,2048]{1,0:T(8,128)(2,1)} %convolution_convert_fusion.1) | data formatting | bytes 5242880 | tf_op jit(solution)/shard_map/reshape | solution.py:164
  188.9 116.0 %all_to_all.29 = bf16[32,20,2048]{2,1,0:T(8,128)(2,1)} all-to-all(bf16[32,20,2048]{2,1,0:T(8,128)(2,1)} %reshape.354), channel_id=1, replica_groups=mesh['sp'=32,'tp'=8] {'sp'}, dimensions={0} | all-to-all | bytes 5242880 | tf_op jit(solution)/shard_map/all_to_all | solution.py:165
  304.9 5.2 %reshape.355 = bf16[640,2048]{1,0:T(8,128)(2,1)} reshape(bf16[32,20,2048]{2,1,0:T(8,128)(2,1)} %all_to_all.29) | data formatting | bytes 5242880 | tf_op jit(solution)/shard_map/reshape | solution.py:166
  310.1 5.0 %fusion.43 = f32[640,512]{1,0:T(8,128)} fusion(bf16[640,2048]{1,0:T(8,128)(2,1)} %reshape.355, bf16[1,2048,512]{2,1,0:T(8,128)(2,1)} %param.41), kind=kOutput, calls=%fused_computation.55 | convolution fusion | flops 1342177280 | bytes 6029312 | tf_op jit(solution)/shard_map/dot_general | solution.py:167
  315.1 7.3 %convolution_convert_fusion = bf16[640,2048]{1,0:T(8,128)(2,1)} fusion(bf16[1,512,2048]{2,1,0:T(8,128)(2,1)S(1)} %copy-done, bf16[640,2048]{1,0:T(8,128)(2,1)} %reshape.355, bf16[1,2048,512]{2,1,0:T(8,128)(2,1)} %param.42, f32[640,512]{1,0:T(8,128)} %fusion.43), kind=kOutput, calls=%fused_computation.47 | convolution fusion | flops 2687631360 | bytes 10747904 | tf_op jit(solution)/shard_map/dot_general | solution.py:170
  322.3 5.1 %reshape.356 = bf16[32,20,2048]{2,1,0:T(8,128)(2,1)} reshape(bf16[640,2048]{1,0:T(8,128)(2,1)} %convolution_convert_fusion) | data formatting | bytes 5242880 | tf_op jit(solution)/shard_map/reshape | solution.py:172
  327.5 5.7 %all-to-all-start.2 = ((bf16[32,20,2048]{2,1,0:T(8,128)(2,1)}), bf16[32,20,2048]{2,1,0:T(8,128)(2,1)}, u32[]{:S(2)}, u32[]{:S(2)}) async-start(bf16[32,20,2048]{2,1,0:T(8,128)(2,1)} %reshape.356), calls=%async_computation.2 | async-start | bytes 6291456 | tf_op jit(solution)/shard_map/all_to_all | solution.py:171
  334.4 69.3 %all-to-all-done.2 = bf16[32,20,2048]{2,1,0:T(8,128)(2,1)} async-done(((bf16[32,20,2048]{2,1,0:T(8,128)(2,1)}), bf16[32,20,2048]{2,1,0:T(8,128)(2,1)}, u32[]{:S(2)}, u32[]{:S(2)}) %all-to-all-start.2) | async-done | bytes 2621472 | tf_op jit(solution)/shard_map/all_to_all | solution.py:171
  403.7 5.2 %reshape.358 = bf16[640,2048,1]{1,0,2:T(8,128)(2,1)} reshape(bf16[32,20,2048]{2,1,0:T(8,128)(2,1)} %all-to-all-done.2) | data formatting | bytes 5242880 | tf_op jit(solution)/shard_map/reshape | solution.py:174
  (144 shorter events, 129.5 us)
Async XLA Ops:
  0.0 315.1 %copy-start = (bf16[1,512,2048]{2,1,0:T(8,128)(2,1)S(1)}, bf16[1,512,2048]{2,1,0:T(8,128)(2,1)}, u32[]{:S(2)}) copy-start(bf16[1,512,2048]{2,1,0:T(8,128)(2,1)} %param.43) | copy-start | bytes 6291460
  1.2 15.6 %collective-permute-start.2 = (bf16[2,1024,128]{2,1,0:T(8,128)(2,1)S(1)}, bf16[2,1024,128]{2,1,0:T(8,128)(2,1)S(1)}, u32[]{:S(2)}, u32[]{:S(2)}) collective-permute-start(bf16[2,1024,128]{2,1,0:T(8,128)(2,1)S(1)} %pad_maximum_fusion), channel_id=1, source_target_pairs={{0,8},{8,16},{16,24},{24,32},{32,40},{40,48},{48,56},{56,64},{64,7... | collective-permute-start | bytes 1572872 | tf_op jit(solution)/shard_map/ppermute | solution.py:17
  18.9 38.8 %collective-permute-start.3 = (bf16[2,2048,128]{2,1,0:T(8,128)(2,1)}, bf16[2,2048,128]{2,1,0:T(8,128)(2,1)}, u32[]{:S(2)}, u32[]{:S(2)}) collective-permute-start(bf16[2,2048,128]{2,1,0:T(8,128)(2,1)} %maximum_maximum_fusion.2), channel_id=1, source_target_pairs={{0,16},{8,24},{16,32},{24,40},{32,48},{40,56},{48,64},{56,72},{64,... | collective-permute-start | bytes 3145736 | tf_op jit(solution)/shard_map/ppermute | solution.py:17
  23.9 26.9 %collective-permute-start.4 = (f32[2,1024]{1,0:T(2,128)}, f32[2,1024]{1,0:T(2,128)}, u32[]{:S(2)}, u32[]{:S(2)}) collective-permute-start(f32[2,1024]{1,0:T(2,128)} %param.34), channel_id=1, source_target_pairs={{0,8},{8,16},{16,24},{24,32},{32,40},{40,48},{48,56},{56,64},{64,7... | collective-permute-start | bytes 24584 | tf_op jit(solution)/shard_map/ppermute | solution.py:17
  28.2 18.8 %collective-permute-start = (s32[1024]{0:T(1024)}, s32[1024]{0:T(1024)}, u32[]{:S(2)}, u32[]{:S(2)}) collective-permute-start(s32[1024]{0:T(1024)} %param.35), channel_id=1, source_target_pairs={{0,8},{8,16},{16,24},{24,32},{32,40},{40,48},{48,56},{56,64},{64,7... | collective-permute-start | bytes 12296 | tf_op jit(solution)/shard_map/ppermute | solution.py:17
  31.2 3.6 copy-start.5
  32.1 28.2 %copy-start.7 = (s32[256]{0:T(256)}, s32[256]{0:T(256)S(1)}, u32[]{:S(2)}) copy-start(s32[256]{0:T(256)S(1)} %fusion.62) | copy-start | bytes 3076
  47.6 15.5 %collective-permute-start.1 = (s32[2048]{0:T(1024)S(1)}, s32[2048]{0:T(1024)}, u32[]{:S(2)}, u32[]{:S(2)}) collective-permute-start(s32[2048]{0:T(1024)S(1)} %pad_add_fusion), channel_id=1, source_target_pairs={{0,16},{8,24},{16,32},{24,40},{32,48},{40,56},{48,64},{56,72},{64,... | collective-permute-start | bytes 24584 | tf_op jit(solution)/shard_map/ppermute | solution.py:17
  51.6 11.6 %collective-permute-start.5 = (f32[2,2048]{1,0:T(2,128)S(1)}, f32[2,2048]{1,0:T(2,128)}, u32[]{:S(2)}, u32[]{:S(2)}) collective-permute-start(f32[2,2048]{1,0:T(2,128)S(1)} %pad_maximum_fusion.1), channel_id=1, source_target_pairs={{0,16},{8,24},{16,32},{24,40},{32,48},{40,56},{48,64},{56,72},{64,... | collective-permute-start | bytes 49160 | tf_op jit(solution)/shard_map/ppermute | solution.py:17
  99.2 0.7 copy-start.1
  106.0 0.7 copy-start.2
  150.2 0.7 copy-start.1
  157.0 0.7 copy-start.2
  165.7 15.5 %copy-start.9 = (f32[2048]{0:T(1024)S(1)}, f32[2048]{0:T(1024)}, u32[]{:S(2)}) copy-start(f32[2048]{0:T(1024)} %param.38) | copy-start | bytes 24580
  165.7 12.1 %all-to-all-start = ((bf16[8,128,128]{2,1,0:T(8,128)(2,1)}), bf16[8,128,128]{2,1,0:T(8,128)(2,1)S(1)}, u32[]{:S(2)}, u32[]{:S(2)}) async-start(bf16[8,128,128]{2,1,0:T(8,128)(2,1)} %bitcast.103), calls=%async_computation | async-start | bytes 524288 | tf_op jit(solution)/shard_map/all_to_all | solution.py:144
  178.0 3.2 copy-start.3
  327.5 5.8 %copy-start.6 = (s32[256]{0:T(256)S(1)}, s32[256]{0:T(256)}, u32[]{:S(2)}) copy-start(s32[256]{0:T(256)} %copy-done.5) | copy-start | bytes 3076
  327.5 5.8 %copy-start.8 = (s32[256]{0:T(256)S(1)}, s32[256]{0:T(256)}, u32[]{:S(2)}) copy-start(s32[256]{0:T(256)} %copy-done.7) | copy-start | bytes 3076
  327.5 76.2 %all-to-all-start.2 = ((bf16[32,20,2048]{2,1,0:T(8,128)(2,1)}), bf16[32,20,2048]{2,1,0:T(8,128)(2,1)}, u32[]{:S(2)}, u32[]{:S(2)}) async-start(bf16[32,20,2048]{2,1,0:T(8,128)(2,1)} %reshape.356), calls=%async_computation.2 | async-start | bytes 6291456 | tf_op jit(solution)/shard_map/all_to_all | solution.py:171
  333.2 75.6 %copy-start.10 = (f32[128,2]{0,1:T(2,128)S(1)}, f32[128,2]{0,1:T(2,128)}, u32[]{:S(2)}) copy-start(f32[128,2]{0,1:T(2,128)} %param.40) | copy-start | bytes 3076
  334.4 74.5 %copy-start.4 = (pred[128,2,640]{2,1,0:T(4,128)(4,1)S(1)}, pred[128,2,640]{2,1,0:T(4,128)(4,1)}, u32[]{:S(2)}) copy-start(pred[128,2,640]{2,1,0:T(4,128)(4,1)} %eq.130) | copy-start | bytes 491524
where the time goes:
time: 410 us; the launch traced here: 413 us
  blocking collectives  116 us (28%)
  waiting for transfers between devices  98.3 us (24%)
  local copies, waits for them, and re-layouts  61 us (15%)
  matrix products  49.7 us (12%)
  starting transfers between devices  34.2 us (8%)
  other arithmetic  28.8 us (7%)
  loops' own time  21.7 us (5%)
    all_to_all x1, blocking collectives, per_device(): lax.all_to_all(sent, 'sp', split_axis=0, concat_axis=0, tiled=True)  116 us
    all_to_all x1, waiting for transfers between devices, per_device(): lax.all_to_all(outcome.reshape(arrived.shape), 'sp', split_axis=0, concat...  69.3 us
    ppermute x6, starting transfers between devices, from_behind(): return lax.ppermute(block, axis, route)  23.9 us
    ppermute x6, waiting for transfers between devices, from_behind(): return lax.ppermute(block, axis, route)  22.9 us
    another operation x1, loops' own time, per_device(): lax.map(attend, jnp.arange(tok_dev // block_rows, dtype=jnp.int32))  21.4 us
    dot_general x4, matrix products, compute(): jnp.einsum('qhd,khd->hqk', query, key_split[lower:lower + tok_dev], prefe...  16.9 us
    reduce_sum x4, other arithmetic, weigh(): return (jnp.sum(expo, axis=-1), product)  12.3 us
    dot_general x4, matrix products, weigh(): jnp.einsum('hqk,khd->qhd', rounded, value_split[lower:lower + tok_dev], p...  12.1 us
  transfers between devices with their start and end apart: 8, of which 4 were waited for; matrix products, arithmetic and copies ran while one was open for 3% of the time, Pallas kernels for 0%

commit v1 on v0

v1 whole, which is shorter than its diff:
```python
import functools
import jax
import jax.numpy as jnp
from jax import lax
from jax.experimental import pallas as pl
from jax.experimental.pallas import tpu as pltpu
from jax.sharding import PartitionSpec as P

EPG = 4
TOPK = 2
REACH = 3
QT = 256
KT = 512
FAR = -1e30

norm_eps = 1e-06
F32 = jnp.float32
BF16 = jnp.bfloat16


def columns_of(rows):
    parts = [jnp.transpose(rows[:, c : c + 128]) for c in range(0, rows.shape[1], 128)]
    return jnp.concatenate(parts, axis=0).astype(BF16)


def mixer_kernel(
    n_sp, n_tp, q_ref, k_ref, v_ref, marks_ref, out_ref,
    kbuf, vbuf, mbuf, qaug, kmark, vaug, top, acc, att, heads,
    ksend, krecv, vsend, vrecv, msend, mrecv, hsend, hrecv,
):
    sp = lax.axis_index("sp")
    tp = lax.axis_index("tp")
    tok = q_ref.shape[0]
    chunk = tok // n_tp

    barrier = pltpu.get_barrier_semaphore()
    for d in range(1, REACH + 1):
        for other in (lax.rem(sp + d, n_sp), lax.rem(sp + n_sp - d, n_sp)):
            pl.semaphore_signal(barrier, inc=1, device_id={"sp": other})
    for d in range(1, n_tp):
        pl.semaphore_signal(barrier, inc=1, device_id={"tp": lax.rem(tp + d, n_tp)})
    pl.semaphore_wait(barrier, 2 * REACH + n_tp - 1)

    halo = []
    for d in range(1, REACH + 1):
        ahead = {"sp": lax.rem(sp + d, n_sp)}
        parts = []
        for src, buf, send, recv in (
            (marks_ref, mbuf, msend, mrecv), (k_ref, kbuf, ksend, krecv), (v_ref, vbuf, vsend, vrecv)
        ):
            copy = pltpu.make_async_remote_copy(
                src_ref=src, dst_ref=buf.at[d - 1], send_sem=send.at[d - 1], recv_sem=recv.at[d - 1],
                device_id=ahead,
            )
            copy.start()
            parts.append(copy)
        halo.append(parts)

    lane = lax.broadcasted_iota(jnp.int32, (1, 128), 1)
    row8 = lax.broadcasted_iota(jnp.int32, (8, tok), 0)
    row16 = lax.broadcasted_iota(jnp.int32, (16, tok), 0).astype(F32)
    blank = jnp.zeros((104, tok), F32)
    own = marks_ref[...]
    base = own[0:2, 0:1]

    same = (own[2:3, :] == row16).astype(F32)
    qmark = columns_of(jnp.concatenate([jnp.zeros((8, tok), F32), same, blank], axis=0))
    qrows = q_ref[...] * jnp.asarray(0.125, BF16)
    for h in range(2):
        mine = (lane >= 64 * h) & (lane < 64 * h + 64)
        ones = (lane >= 3 * h) & (lane < 3 * h + 3)
        qaug[h, :, 0:128] = jnp.where(mine, qrows, jnp.zeros_like(qrows))
        qaug[h, :, 128:256] = jnp.where(ones, jnp.ones_like(qmark), qmark)

    def prepare(marks, v):
        gate = base - marks[0:2, :]
        high = gate.astype(BF16).astype(F32)
        rest = gate - high
        mid = rest.astype(BF16).astype(F32)
        low = rest - mid
        pieces = jnp.zeros((8, tok), F32)
        for h in range(2):
            for i, piece in enumerate((high, mid, low)):
                pieces = jnp.where(row8 == 3 * h + i, piece[h : h + 1, :], pieces)
        other = jnp.where(marks[2:3, :] == row16, 0.0, FAR).astype(F32)
        kmark[...] = columns_of(jnp.concatenate([pieces, other, blank], axis=0))
        one = jnp.ones_like(v)
        vaug[0] = jnp.where(lane < 64, v, one)
        vaug[1] = jnp.where(lane < 64, one, v)

    def tile(keys, q0, k0, fresh, causal):
        rows = pl.ds(q0, QT)
        kk = jnp.concatenate([keys[pl.ds(k0, KT), :], kmark[pl.ds(k0, KT), :]], axis=1)
        for h in range(2):
            score = lax.dot_general(
                qaug[h, rows, :], kk, (((1,), (1,)), ((), ())), preferred_element_type=F32
            )
            if causal:
                qpos = q0 + lax.broadcasted_iota(jnp.int32, (QT, KT), 0)
                kpos = k0 + lax.broadcasted_iota(jnp.int32, (QT, KT), 1)
                score = jnp.where(kpos <= qpos, score, FAR)
            best = jnp.broadcast_to(jnp.max(score, axis=1, keepdims=True), (QT, 128))
            if not fresh:
                old = top[h, rows, :]
                best = jnp.maximum(best, old)
            expo = jnp.exp(score - jnp.concatenate([best] * (KT // 128), axis=1)).astype(BF16)
            part = jnp.dot(expo, vaug[h, pl.ds(k0, KT), :], preferred_element_type=F32)
            if not fresh:
                part = acc[h, rows, :] * jnp.exp(old - best) + part
            top[h, rows, :] = best
            acc[h, rows, :] = part

    prepare(own, v_ref[...])
    tiles = tok // QT
    per = KT // QT
    for k0 in range(0, tok, KT):
        first = k0 // QT

        def diagonal(i, carry, k0=k0):
            tile(k_ref, pl.multiple_of(i * QT, QT), k0, k0 == 0, True)
            return carry

        def below(i, carry, k0=k0):
            tile(k_ref, pl.multiple_of(i * QT, QT), k0, k0 == 0, False)
            return carry

        lax.fori_loop(first, first + per, diagonal, 0)
        if first + per < tiles:
            lax.fori_loop(first + per, tiles, below, 0)

    for d in range(1, REACH + 1):
        for copy in halo[d - 1]:
            copy.wait_recv()
        prepare(mbuf[d - 1], vbuf[d - 1])
        keys = kbuf.at[d - 1]
        if d < REACH:

            def full(i, carry, keys=keys):
                for k0 in range(0, tok, KT):
                    tile(keys, pl.multiple_of(i * QT, QT), k0, False, False)
                return carry

            lax.fori_loop(0, tiles, full, 0)

    keys = kbuf.at[REACH - 1]
    sends = []
    for i in range(tiles):
        q0 = i * QT
        for k0 in range(q0 // KT * KT, tok, KT):
            tile(keys, q0, k0, False, False)
        rows = pl.ds(q0, QT)
        total = jnp.where(lane < 64, pltpu.roll(acc[0, rows, :], 64, 1), pltpu.roll(acc[1, rows, :], 64, 1))
        value = jnp.where(lane < 64, acc[0, rows, :], acc[1, rows, :])
        att[rows, :] = (value / total).astype(BF16)
        for c in range(q0 // chunk, (q0 + QT) // chunk):

            @pl.when(tp != c)
            def _(c=c):
                pltpu.make_async_remote_copy(
                    src_ref=att.at[pl.ds(c * chunk, chunk)], dst_ref=heads.at[tp],
                    send_sem=hsend.at[c], recv_sem=hrecv.at[tp], device_id={"tp": c},
                ).start()

    for c in range(n_tp):

        @pl.when(tp != c)
        def _(c=c):
            pltpu.make_async_remote_copy(
                src_ref=att.at[pl.ds(c * chunk, chunk)], dst_ref=heads.at[c],
                send_sem=hsend.at[c], recv_sem=hrecv.at[c], device_id={"tp": c},
            ).wait_recv()
            out_ref[:, c * 128 : (c + 1) * 128] = heads[c]

        @pl.when(tp == c)
        def _(c=c):
            out_ref[:, c * 128 : (c + 1) * 128] = att[c * chunk : (c + 1) * chunk, :]

    for c in range(n_tp):

        @pl.when(tp != c)
        def _(c=c):
            pltpu.make_async_remote_copy(
                src_ref=att.at[pl.ds(c * chunk, chunk)], dst_ref=heads.at[c],
                send_sem=hsend.at[c], recv_sem=hrecv.at[c], device_id={"tp": c},
            ).wait_send()

    for parts in halo:
        for copy in parts:
            copy.wait_send()


def mixer(query_rows, key_rows, value_rows, forget_cum, doc_ids):
    n_sp, n_tp = lax.axis_size("sp"), lax.axis_size("tp")
    tok, width = query_rows.shape
    marks = jnp.concatenate(
        [forget_cum, doc_ids.astype(F32)[None, :], jnp.zeros((5, tok), F32)], axis=0
    )
    vmem = pl.BlockSpec(memory_space=pltpu.VMEM)
    dma = pltpu.SemaphoreType.DMA
    return pl.pallas_call(
        functools.partial(mixer_kernel, n_sp, n_tp),
        out_shape=jax.ShapeDtypeStruct((tok // n_tp, width * n_tp), BF16),
        in_specs=[vmem] * 4,
        out_specs=vmem,
        scratch_shapes=[
            pltpu.VMEM((REACH, tok, width), BF16),
            pltpu.VMEM((REACH, tok, width), BF16),
            pltpu.VMEM((REACH, 8, tok), F32),
            pltpu.VMEM((2, tok, 2 * width), BF16),
            pltpu.VMEM((tok, width), BF16),
            pltpu.VMEM((2, tok, width), BF16),
            pltpu.VMEM((2, tok, 128), F32),
            pltpu.VMEM((2, tok, 128), F32),
            pltpu.VMEM((tok, width), BF16),
            pltpu.VMEM((n_tp, tok // n_tp, width), BF16),
            dma((REACH,)), dma((REACH,)), dma((REACH,)), dma((REACH,)), dma((REACH,)), dma((REACH,)),
            dma((n_tp,)), dma((n_tp,)),
        ],
        compiler_params=pltpu.CompilerParams(
            collective_id=0, has_side_effects=True, vmem_limit_bytes=48 * 1024 * 1024
        ),
        name="mixer",
    )(query_rows, key_rows, value_rows, marks)


def per_device(
    query_rows,
    key_rows,
    value_rows,
    forget_cum,
    doc_ids,
    residual,
    out_weight,
    norm_gain,
    expert_ids,
    route_weights,
    gate_proj,
    up_proj,
    down_proj,
):
    tok_loc = residual.shape[0]
    token_heads = mixer(query_rows, key_rows, value_rows, forget_cum, doc_ids)
    mixed = jnp.dot(token_heads, out_weight, preferred_element_type=jnp.float32)
    hidden = residual.astype(jnp.float32) + mixed
    normed = (
        hidden * lax.rsqrt(jnp.mean(hidden * hidden, axis=-1, keepdims=True) + norm_eps) * norm_gain
    ).astype(jnp.bfloat16)
    experts = lax.axis_size("sp")
    groups = experts // EPG
    capacity = max(2, 5 * tok_loc // (4 * groups))
    width = normed.shape[1]
    flat = expert_ids.reshape(-1)
    onehot = (flat[:, None] == jnp.arange(experts, dtype=jnp.int32)[None, :]).astype(jnp.int32)
    earlier = jnp.cumsum(onehot, axis=0) - onehot
    slot_rank = jnp.sum(earlier * onehot, axis=1)
    slot = flat * capacity + slot_rank
    select = (jnp.arange(experts * capacity, dtype=jnp.int32)[:, None] == slot[None, :]).astype(
        jnp.bfloat16
    )
    select_tokens = select.reshape(experts * capacity, tok_loc, TOPK).sum(axis=-1)
    sent = jnp.dot(select_tokens, normed, preferred_element_type=jnp.float32).astype(jnp.bfloat16)
    sent = sent.reshape(experts, capacity, width)
    arrived = lax.all_to_all(sent, "sp", split_axis=0, concat_axis=0, tiled=True)
    rows = arrived.reshape(-1, width)
    gate = jnp.dot(rows, gate_proj[0], preferred_element_type=jnp.float32)
    up = jnp.dot(rows, up_proj[0], preferred_element_type=jnp.float32)
    act = (jax.nn.silu(gate) * up).astype(jnp.bfloat16)
    outcome = jnp.dot(act, down_proj[0], preferred_element_type=jnp.float32).astype(jnp.bfloat16)
    back = lax.all_to_all(
        outcome.reshape(arrived.shape), "sp", split_axis=0, concat_axis=0, tiled=True
    )
    back_rows = back.reshape(experts * capacity, width)
    picked = lax.dot_general(
        select, back_rows, (((0,), (0,)), ((), ())), preferred_element_type=jnp.float32
    )
    picked = picked.reshape(tok_loc, TOPK, width)
    combined = jnp.sum(picked * route_weights[:, :, None], axis=1)
    return (hidden + combined).astype(jnp.bfloat16)


def solution(mesh):
    placed = (
        P("sp", "tp"),
        P("sp", "tp"),
        P("sp", "tp"),
        P("tp", "sp"),
        P("sp"),
        P(("sp", "tp"), None),
        P(),
        P(),
        P(("sp", "tp"), None),
        P(("sp", "tp"), None),
        P("sp", None, None),
        P("sp", None, None),
        P("sp", None, None),
    )
    return jax.shard_map(
        per_device, mesh=mesh, in_specs=placed, out_specs=P(("sp", "tp"), None), check_vma=False
    )
```

time: 410 us -> 282 us (0.69); the launches traced: 413 us -> 279 us
  Pallas kernels: 0 us -> 68.7 us
  local copies, waits for them, and re-layouts: 61 us -> 26.2 us
  blocking collectives: 116 us -> 83 us
  matrix products: 49.7 us -> 20.7 us
  starting transfers between devices: 34.2 us -> 5.61 us
  waiting for transfers between devices: 98.3 us -> 70.4 us
  other arithmetic: 28.8 us -> 4.08 us
  loops' own time: 21.7 us -> 0 us
    pallas_call x0 -> x1, Pallas kernels: none -> 68.7 us  [mixer(): pl.pallas_call(functools.partial(mixer_kernel, n_sp, n_tp), out_shape=jax...]
    all_to_all x1, blocking collectives: 116 us -> 83 us  [per_device(): lax.all_to_all(sent, 'sp', split_axis=0, concat_axis=0, tiled=True)]
    dot_general x8 -> x0, matrix products: 29 us -> none  [the longest x4 16.9 us: compute(): jnp.einsum('qhd,khd->hqk', query, key_split[lower:lower + tok_dev], prefe...]
    ppermute x6 -> x0, starting transfers between devices: 23.9 us -> none  [from_behind(): return lax.ppermute(block, axis, route)]
    ppermute x6 -> x0, waiting for transfers between devices: 22.9 us -> none  [from_behind(): return lax.ppermute(block, axis, route)]
    another operation x17 -> x0, loops' own time: 21.7 us -> none  [the longest x1 21.4 us: per_device(): lax.map(attend, jnp.arange(tok_dev // block_rows, dtype=jnp.int32))]
    slice x19 -> x1, local copies, waits for them, and re-layouts: 15 us -> 0.18 us  [the longest x4 5.17 us: attend(): key_doc[-1] >= query_doc[0]]
    reduce_sum x4 -> x0, other arithmetic: 12.3 us -> none  [weigh(): return (jnp.sum(expo, axis=-1), product)]
  transfers between devices with their start and end apart: 8 -> 1, of which waited for: 4 -> 1; matrix products, arithmetic and copies ran while one was open for 3% -> 0% of each run, Pallas kernels for 0% -> 0%
where the time goes in v1:
time: 282 us; the launch traced here: 279 us
  blocking collectives  83 us (29%)
  waiting for transfers between devices  70.4 us (25%)
  Pallas kernels  68.7 us (24%)
  local copies, waits for them, and re-layouts  26.2 us (9%)
  matrix products  20.7 us (7%)
  starting transfers between devices  5.61 us (2%)
  other arithmetic  4.08 us (1%)
    all_to_all x1, blocking collectives, per_device(): lax.all_to_all(sent, 'sp', split_axis=0, concat_axis=0, tiled=True)  83 us
    all_to_all x1, waiting for transfers between devices, per_device(): lax.all_to_all(outcome.reshape(arrived.shape), 'sp', split_axis=0, concat...  70.4 us
    pallas_call x1, Pallas kernels, mixer(): pl.pallas_call(functools.partial(mixer_kernel, n_sp, n_tp), out_shape=jax...  68.7 us
    dot_general x1, matrix products, per_device(): jnp.dot(act, down_proj[0], preferred_element_type=jnp.float32)  7.23 us
  transfers between devices with their start and end apart: 1, of which 1 were waited for; matrix products, arithmetic and copies ran while one was open for 0% of the time, Pallas kernels for 0%

profile of v1, /device:TPU:2, one launch (start us, length us, event | category | flops | bytes accessed | tf_op | source)
XLA Modules:
  0.0 278.8 jit_solution(10093800605756771343)
XLA Ops:
  0.0 0.9 copy.28
  1.2 0.6 reduce-window.6
  1.8 0.2 slice_reduce_fusion
  2.4 0.7 multiply_add_fusion
  3.2 0.7 convert_element_type.35
  3.9 0.8 maximum_maximum_fusion.marks_ref
  4.7 0.9 copy-done.1
  5.6 0.9 copy-done.2
  6.6 0.9 copy-done.3
  7.5 68.7 %mixer.1 = bf16[128,1024]{1,0:T(8,128)(2,1)S(1)} custom-call(bf16[1024,128]{1,0:T(8,128)(2,1)S(1)} %copy-done.1, bf16[1024,128]{1,0:T(8,128)(2,1)S(1)} %copy-done.2, bf16[1024,128]{1,0:T(8,128)(2,1)S(1)} %copy-done.3, f32[8,1024]{1,0:T(8,128)S(1)} %maximum_maximum_fusion.marks_ref), custom_call_target="tpu_custom_call" | custom-call | tf_op jit(solution)/shard_map/mixer/pallas_call | solution.py:200
  76.3 3.1 %multiply_reduce_fusion = (f32[128]{0:T(128)S(1)}, f32[128,2048]{1,0:T(8,128)S(1)}) fusion(bf16[128,1024]{1,0:T(8,128)(2,1)S(1)} %mixer.1, bf16[1024,2048]{1,0:T(8,128)(2,1)} %param.19, bf16[128,2048]{1,0:T(8,128)(2,1)} %param.18), kind=kOutput, calls=%fused_computation.14 | convolution fusion | flops 537919360 | bytes 6029824 | tf_op jit(solution)/shard_map/dot_general | solution.py:243
  79.5 2.4 convolution_convert_fusion.1
  81.9 5.2 %reshape.88 = bf16[32,20,2048]{2,1,0:T(8,128)(2,1)} reshape(bf16[640,2048]{1,0:T(8,128)(2,1)} %convolution_convert_fusion.1) | data formatting | bytes 5242880 | tf_op jit(solution)/shard_map/reshape | solution.py:262
  87.1 83.0 %all_to_all.10 = bf16[32,20,2048]{2,1,0:T(8,128)(2,1)} all-to-all(bf16[32,20,2048]{2,1,0:T(8,128)(2,1)} %reshape.88), channel_id=1, replica_groups=mesh['sp'=32,'tp'=8] {'sp'}, dimensions={0} | all-to-all | bytes 5242880 | tf_op jit(solution)/shard_map/all_to_all | solution.py:263
  170.1 5.2 %reshape.89 = bf16[640,2048]{1,0:T(8,128)(2,1)} reshape(bf16[32,20,2048]{2,1,0:T(8,128)(2,1)} %all_to_all.10) | data formatting | bytes 5242880 | tf_op jit(solution)/shard_map/reshape | solution.py:264
  175.3 5.0 %fusion.3 = f32[640,512]{1,0:T(8,128)} fusion(bf16[640,2048]{1,0:T(8,128)(2,1)} %reshape.89, bf16[1,2048,512]{2,1,0:T(8,128)(2,1)} %param.23), kind=kOutput, calls=%fused_computation.7 | convolution fusion | flops 1342177280 | bytes 6029312 | tf_op jit(solution)/shard_map/dot_general | solution.py:265
  180.3 7.2 %convolution_convert_fusion = bf16[640,2048]{1,0:T(8,128)(2,1)} fusion(bf16[1,512,2048]{2,1,0:T(8,128)(2,1)S(1)} %copy-done, bf16[640,2048]{1,0:T(8,128)(2,1)} %reshape.89, bf16[1,2048,512]{2,1,0:T(8,128)(2,1)} %param.24, f32[640,512]{1,0:T(8,128)} %fusion.3), kind=kOutput, calls=%fused_computation | convolution fusion | flops 2687631360 | bytes 10747904 | tf_op jit(solution)/shard_map/dot_general | solution.py:268
  187.5 5.2 %reshape.90 = bf16[32,20,2048]{2,1,0:T(8,128)(2,1)} reshape(bf16[640,2048]{1,0:T(8,128)(2,1)} %convolution_convert_fusion) | data formatting | bytes 5242880 | tf_op jit(solution)/shard_map/reshape | solution.py:270
  192.7 5.6 %all-to-all-start.1 = ((bf16[32,20,2048]{2,1,0:T(8,128)(2,1)}), bf16[32,20,2048]{2,1,0:T(8,128)(2,1)}, u32[]{:S(2)}, u32[]{:S(2)}) async-start(bf16[32,20,2048]{2,1,0:T(8,128)(2,1)} %reshape.90), calls=%async_computation.1 | async-start | bytes 6291456 | tf_op jit(solution)/shard_map/all_to_all | solution.py:269
  198.5 0.9 eq.62
  199.4 70.4 %all-to-all-done.1 = bf16[32,20,2048]{2,1,0:T(8,128)(2,1)} async-done(((bf16[32,20,2048]{2,1,0:T(8,128)(2,1)}), bf16[32,20,2048]{2,1,0:T(8,128)(2,1)}, u32[]{:S(2)}, u32[]{:S(2)}) %all-to-all-start.1) | async-done | bytes 2621472 | tf_op jit(solution)/shard_map/all_to_all | solution.py:269
  269.8 5.2 %reshape.92 = bf16[640,2048,1]{1,0,2:T(8,128)(2,1)} reshape(bf16[32,20,2048]{2,1,0:T(8,128)(2,1)} %all-to-all-done.1) | data formatting | bytes 5242880 | tf_op jit(solution)/shard_map/reshape | solution.py:272
  275.0 2.8 %fusion.5 = f32[128,2048]{1,0:T(8,128)S(1)} fusion(bf16[640,2048,1]{1,0,2:T(8,128)(2,1)} %reshape.92, f32[128,2]{0,1:T(2,128)S(1)} %copy-done.6, pred[128,2,640]{2,1,0:T(4,128)(4,1)S(1)} %copy-done.4), kind=kOutput, calls=%fused_computation.9 | convolution fusion | flops 671875072 | bytes 3834880 | tf_op jit(solution)/shard_map/dot_general | solution.py:273
  277.9 0.9 add_convert_fusion
  (25 shorter events, 1.0 us)
Async XLA Ops:
  0.0 180.3 %copy-start = (bf16[1,512,2048]{2,1,0:T(8,128)(2,1)S(1)}, bf16[1,512,2048]{2,1,0:T(8,128)(2,1)}, u32[]{:S(2)}) copy-start(bf16[1,512,2048]{2,1,0:T(8,128)(2,1)} %param.25) | copy-start | bytes 6291460
  4.7 0.9 copy-start.1
  5.6 0.9 copy-start.2
  6.6 0.9 copy-start.3
  76.3 3.2 %copy-start.5 = (f32[2048]{0:T(1024)S(1)}, f32[2048]{0:T(1024)}, u32[]{:S(2)}) copy-start(f32[2048]{0:T(1024)} %param.20) | copy-start | bytes 24580
  192.7 77.1 %all-to-all-start.1 = ((bf16[32,20,2048]{2,1,0:T(8,128)(2,1)}), bf16[32,20,2048]{2,1,0:T(8,128)(2,1)}, u32[]{:S(2)}, u32[]{:S(2)}) async-start(bf16[32,20,2048]{2,1,0:T(8,128)(2,1)} %reshape.90), calls=%async_computation.1 | async-start | bytes 6291456 | tf_op jit(solution)/shard_map/all_to_all | solution.py:269
  199.4 75.6 %copy-start.4 = (pred[128,2,640]{2,1,0:T(4,128)(4,1)S(1)}, pred[128,2,640]{2,1,0:T(4,128)(4,1)}, u32[]{:S(2)}) copy-start(pred[128,2,640]{2,1,0:T(4,128)(4,1)} %eq.62) | copy-start | bytes 491524
  199.4 75.6 %copy-start.6 = (f32[128,2]{0,1:T(2,128)S(1)}, f32[128,2]{0,1:T(2,128)}, u32[]{:S(2)}) copy-start(f32[128,2]{0,1:T(2,128)} %param.22) | copy-start | bytes 3076

commit v2 on v1

--- a/solution.py
+++ b/solution.py
@@ -223,6 +223,311 @@
     )(query_rows, key_rows, value_rows, marks)
 
 
+HOPS = (0, 1, 7, 2, 6, 3, 5, 4)
+PAIRS = len(HOPS) // 2
+
+
+def stack(blocks):
+    parts = []
+    for block in blocks:
+        parts += [block.astype(F32), jnp.zeros((64 - block.shape[0], block.shape[1]), F32)]
+    return jnp.concatenate(parts, axis=0).astype(BF16)
+
+
+def expert_kernel(
+    capacity, heads_ref, residual_ref, gain_ref, route_ref, mix_hbm, gate_hbm, up_hbm, down_hbm, out_ref,
+    mix, wgate, wup, wdown, hidden, normed, zs, zbuf, ms, mbuf, mcol, xs, xbuf, ys, ybuf, cs, cbuf,
+    load, zsend, zrecv, msend, mrecv, xsend, xrecv, ysend, yrecv, csend, crecv,
+):
+    sp = lax.axis_index("sp")
+    x = lax.rem(sp, EPG)
+    z = sp // EPG
+    planes = len(HOPS)
+    group = 2 * capacity
+    tok, width = residual_ref.shape
+    ffe = wgate.shape[1]
+
+    def along_z(hop):
+        return {"sp": lax.rem(z + hop, planes) * EPG + x}
+
+    def along_x(hop):
+        return {"sp": z * EPG + lax.rem(x + hop, EPG)}
+
+    barrier = pltpu.get_barrier_semaphore()
+    for hop in range(1, planes):
+        pl.semaphore_signal(barrier, inc=1, device_id=along_z(hop))
+    for hop in range(1, EPG):
+        pl.semaphore_signal(barrier, inc=1, device_id=along_x(hop))
+
+    loads = [
+        pltpu.make_async_copy(src, dst, load.at[i])
+        for i, (src, dst) in enumerate(
+            ((mix_hbm, mix), (gate_hbm, wgate), (up_hbm, wup), (down_hbm, wdown))
+        )
+    ]
+    for copy in loads:
+        copy.start()
+
+    ids = route_ref[0:2, :].astype(jnp.int32)
+    id0, id1 = ids[0:1, :], ids[1:2, :]
+    earlier = (
+        lax.broadcasted_iota(jnp.int32, (tok, tok), 0) < lax.broadcasted_iota(jnp.int32, (tok, tok), 1)
+    ).astype(BF16)
+    number = lax.broadcasted_iota(jnp.int32, (planes * EPG, tok), 0)
+    uses = ((number == id0) | (number == id1)).astype(F32)
+    rank = jnp.dot(uses.astype(BF16), earlier, preferred_element_type=F32)
+    row = lax.broadcasted_iota(jnp.int32, (16, tok), 0)
+    which = lax.rem(x + row, EPG)
+    pick = (
+        (lax.broadcasted_iota(jnp.int32, (16, planes * EPG), 1) & (EPG - 1))
+        == lax.rem(x + lax.broadcasted_iota(jnp.int32, (16, planes * EPG), 0), EPG)
+    ).astype(BF16)
+    slots = jnp.dot(pick, (uses * (rank + 1.0)).astype(BF16), preferred_element_type=F32)
+    weight = jnp.where((id0 & (EPG - 1)) == which, route_ref[2:3, :], 0.0) + jnp.where(
+        (id1 & (EPG - 1)) == which, route_ref[3:4, :], 0.0
+    )
+    high = weight.astype(BF16).astype(F32)
+    info = jnp.where(row < 4, slots, jnp.where(row < 8, high, jnp.where(row < 12, weight - high, 0.0)))
+    info = info.astype(BF16)
+    mine = lax.shift_right_logical(id0, 2)
+    member = (lax.broadcasted_iota(jnp.int32, (planes, tok), 0) == mine).astype(F32)
+    place = jnp.sum(
+        member * jnp.dot(member.astype(BF16), earlier, preferred_element_type=F32), axis=0, keepdims=True
+    )
+    mine = mine.astype(F32)
+    spot = lax.broadcasted_iota(jnp.int32, (group, tok), 0).astype(F32)
+    sel = []
+    for hop in HOPS:
+        there = lax.rem(z + hop, planes).astype(F32)
+        sel.append(jnp.where((mine == there) & (place == spot), 1.0, 0.0))
+    for s in range(planes):
+        table = lax.dot_general(
+            info, sel[s].astype(BF16), (((1,), (1,)), ((), ())), preferred_element_type=F32
+        )
+        rest = jnp.zeros((16, 64 - group), F32)
+        table = [table, rest, jnp.zeros((16, 64), F32)] if s % 2 == 0 else [jnp.zeros((16, 64), F32), table, rest]
+        table = jnp.concatenate(table, axis=1)
+        if s == 0:
+            mbuf[0] = table
+        else:
+            ms[s] = table
+    sel = jnp.concatenate(sel, axis=0).astype(BF16)
+    wide = lax.broadcasted_iota(jnp.int32, (tok, tok), 0)
+    cols = jnp.transpose(jnp.where(wide == 0, mine, jnp.where(wide == 1, place, 0.0)))
+
+    loads[0].wait()
+    square = jnp.zeros((tok, 128), F32)
+    for c in range(0, width, 512):
+        part = jnp.dot(heads_ref[...], mix[:, c : c + 512], preferred_element_type=F32)
+        part = part + residual_ref[:, c : c + 512].astype(F32)
+        hidden[:, c : c + 512] = part
+        for i in range(0, 512, 128):
+            square = square + part[:, i : i + 128] * part[:, i : i + 128]
+    scale = lax.rsqrt(jnp.sum(square, axis=1, keepdims=True) / width + norm_eps)
+    for c in range(0, width, 512):
+        normed[:, c : c + 512] = (
+            hidden[:, c : c + 512] * scale * gain_ref[:, c : c + 512]
+        ).astype(BF16)
+
+    for c in range(0, width, 512):
+        part = jnp.dot(sel, normed[:, c : c + 512], preferred_element_type=F32)
+        zbuf[0, :, c : c + 512] = part[0:group].astype(BF16)
+        for s in range(1, planes):
+            zs[s, :, c : c + 512] = part[s * group : (s + 1) * group].astype(BF16)
+    pl.semaphore_wait(barrier, planes + EPG - 2)
+
+    def zcopy(s):
+        return pltpu.make_async_remote_copy(
+            src_ref=zs.at[s], dst_ref=zbuf.at[s], send_sem=zsend.at[s], recv_sem=zrecv.at[s],
+            device_id=along_z(HOPS[s]),
+        )
+
+    def mcopy(s):
+        return pltpu.make_async_remote_copy(
+            src_ref=ms.at[s], dst_ref=mbuf.at[s], send_sem=msend.at[s], recv_sem=mrecv.at[s],
+            device_id=along_z(HOPS[s]),
+        )
+
+    def xcopy(p, hop):
+        return pltpu.make_async_remote_copy(
+            src_ref=xs.at[p, hop], dst_ref=xbuf.at[p, hop], send_sem=xsend.at[p, hop],
+            recv_sem=xrecv.at[p, hop], device_id=along_x(hop),
+        )
+
+    def ycopy(p, hop):
+        return pltpu.make_async_remote_copy(
+            src_ref=ys.at[p, hop], dst_ref=ybuf.at[p, hop], send_sem=ysend.at[p, hop],
+            recv_sem=yrecv.at[p, hop], device_id=along_x(EPG - hop),
+        )
+
+    def ccopy(s):
+        return pltpu.make_async_remote_copy(
+            src_ref=cs.at[s], dst_ref=cbuf.at[s], send_sem=csend.at[s], recv_sem=crecv.at[s],
+            device_id=along_z(planes - HOPS[s]),
+        )
+
+    for s in range(1, planes):
+        mcopy(s).start()
+        zcopy(s).start()
+
+    def spread(p):
+        for half in range(2):
+            s = 2 * p + half
+            if s:
+                mcopy(s).wait_recv()
+            table = jnp.concatenate([mbuf[s], jnp.zeros((112, 128), F32)], axis=0)
+            mcol[s] = jnp.transpose(table)[64 * half : 64 * half + group, :]
+        second = mbuf[2 * p + 1]
+        table = mbuf[2 * p] + jnp.where(second > 0.0, second + float(capacity), 0.0)
+        want = lax.broadcasted_iota(jnp.int32, (group, 128), 0).astype(F32) + 1.0
+        rows = [jnp.where(table[h : h + 1, :] == want, 1.0, 0.0) for h in range(EPG)]
+        order = jnp.concatenate(rows, axis=0).astype(BF16)
+        for half in range(2):
+            if 2 * p + half:
+                zcopy(2 * p + half).wait_recv()
+        for c in range(0, width, 512):
+            rows = stack([zbuf[2 * p, :, c : c + 512], zbuf[2 * p + 1, :, c : c + 512]])
+            part = jnp.dot(order, rows, preferred_element_type=F32)
+            xbuf[p, 0, :, c : c + 512] = part[0:group].astype(BF16)
+            for h in range(1, EPG):
+                xs[p, h, :, c : c + 512] = part[h * group : (h + 1) * group].astype(BF16)
+        for h in range(1, EPG):
+            xcopy(p, h).start()
+
+    def expert(p):
+        for h in range(1, EPG):
+            xcopy(p, h).wait_recv()
+        gate = jnp.zeros((EPG * group, ffe), F32)
+        up = jnp.zeros((EPG * group, ffe), F32)
+        for c in range(0, width, 512):
+            rows = jnp.concatenate(
+                [xbuf[p, h, :, c : c + 512].astype(F32) for h in range(EPG)], axis=0
+            ).astype(BF16)
+            gate = gate + jnp.dot(rows, wgate[c : c + 512, :], preferred_element_type=F32)
+            up = up + jnp.dot(rows, wup[c : c + 512, :], preferred_element_type=F32)
+        act = (gate / (1.0 + jnp.exp(-gate)) * up).astype(BF16)
+        for c in range(0, width, 512):
+            part = jnp.dot(act, wdown[:, c : c + 512], preferred_element_type=F32)
+            ybuf[p, 0, :, c : c + 512] = part[0:group].astype(BF16)
+            for h in range(1, EPG):
+                ys[p, h, :, c : c + 512] = part[h * group : (h + 1) * group].astype(BF16)
+        for h in range(1, EPG):
+            ycopy(p, h).start()
+
+    def collect(p):
+        lanes = lax.broadcasted_iota(jnp.int32, (group, 128), 1)
+        left = lanes < 64
+        want = ((lanes & 63) + 1).astype(F32)
+        mats = []
+        for h in range(0, EPG, 2):
+            parts = []
+            for kind in (4, 8):
+                for half in range(2):
+                    col = mcol[2 * p + half]
+                    goal = jnp.where(left, col[:, h : h + 1], col[:, h + 1 : h + 2])
+                    goal = jnp.where(goal > 0.0, goal + float(half * capacity), 0.0)
+                    share = jnp.where(left, col[:, kind + h : kind + h + 1], col[:, kind + h + 1 : kind + h + 2])
+                    parts.append(jnp.where(goal == want, share, 0.0))
+            mats.append(jnp.concatenate(parts, axis=0))
+        mats = jnp.concatenate(mats, axis=1).astype(BF16)
+        for h in range(1, EPG):
+            ycopy(p, h).wait_recv()
+        for c in range(0, width, 512):
+            rows = stack([ybuf[p, h, :, c : c + 512] for h in range(EPG)])
+            part = jnp.dot(mats, rows, preferred_element_type=F32)
+            for half in range(2):
+                both = part[half * group : (half + 1) * group] + part[(2 + half) * group : (3 + half) * group]
+                s = 2 * p + half
+                if s:
+                    cs[s, :, c : c + 512] = both.astype(BF16)
+                else:
+                    cbuf[0, :, c : c + 512] = both.astype(BF16)
+        for half in range(2):
+            if 2 * p + half:
+                ccopy(2 * p + half).start()
+
+    spread(0)
+    spread(1)
+    for copy in loads[1:]:
+        copy.wait()
+    expert(0)
+    spread(2)
+    expert(1)
+    collect(0)
+    spread(3)
+    expert(2)
+    collect(1)
+    expert(3)
+    collect(2)
+    collect(3)
+    lanes = lax.broadcasted_iota(jnp.int32, (tok, 128), 1)
+    back = []
+    for p in range(PAIRS):
+        there = jnp.where(lanes < 64, lax.rem(z + HOPS[2 * p], planes), lax.rem(z + HOPS[2 * p + 1], planes))
+        hit = (cols[:, 0:1] == there.astype(F32)) & (cols[:, 1:2] == (lanes & 63).astype(F32))
+        back.append(jnp.where(hit, 1.0, 0.0))
+    back = jnp.concatenate(back, axis=1).astype(BF16)
+    for s in range(1, planes):
+        ccopy(s).wait_recv()
+    for c in range(0, width, 512):
+        rows = stack([cbuf[s, :, c : c + 512] for s in range(planes)])
+        part = jnp.dot(back, rows, preferred_element_type=F32)
+        out_ref[:, c : c + 512] = (hidden[:, c : c + 512] + part).astype(BF16)
+
+    for s in range(1, planes):
+        mcopy(s).wait_send()
+        zcopy(s).wait_send()
+        ccopy(s).wait_send()
+    for p in range(PAIRS):
+        for h in range(1, EPG):
+            xcopy(p, h).wait_send()
+            ycopy(p, h).wait_send()
+
+
+def experts_layer(heads, residual, out_weight, norm_gain, expert_ids, route_weights, gate, up, down):
+    tok, width = residual.shape
+    ffe = gate.shape[1]
+    planes = lax.axis_size("sp") // EPG
+    capacity = max(2, 5 * tok // (4 * planes))
+    group = 2 * capacity
+    route = jnp.concatenate(
+        [expert_ids.T.astype(F32), route_weights.T, jnp.zeros((4, tok), F32)], axis=0
+    )
+    vmem = pl.BlockSpec(memory_space=pltpu.VMEM)
+    hbm = pl.BlockSpec(memory_space=pl.ANY)
+    dma = pltpu.SemaphoreType.DMA
+    slots = pltpu.VMEM((planes, group, width), BF16)
+    quads = pltpu.VMEM((PAIRS, EPG, group, width), BF16)
+    return pl.pallas_call(
+        functools.partial(expert_kernel, capacity),
+        out_shape=jax.ShapeDtypeStruct((tok, width), BF16),
+        in_specs=[vmem] * 4 + [hbm] * 4,
+        out_specs=vmem,
+        scratch_shapes=[
+            pltpu.VMEM(out_weight.shape, BF16),
+            pltpu.VMEM(gate.shape, BF16),
+            pltpu.VMEM(up.shape, BF16),
+            pltpu.VMEM(down.shape, BF16),
+            pltpu.VMEM((tok, width), F32),
+            pltpu.VMEM((tok, width), BF16),
+            slots, slots,
+            pltpu.VMEM((planes, 16, 128), F32),
+            pltpu.VMEM((planes, 16, 128), F32),
+            pltpu.VMEM((planes, group, 128), F32),
+            quads, quads, quads, quads,
+            slots, slots,
+            dma((4,)),
+            dma((planes,)), dma((planes,)), dma((planes,)), dma((planes,)),
+            dma((PAIRS, EPG)), dma((PAIRS, EPG)), dma((PAIRS, EPG)), dma((PAIRS, EPG)),
+            dma((planes,)), dma((planes,)),
+        ],
+        compiler_params=pltpu.CompilerParams(
+            collective_id=1, has_side_effects=True, vmem_limit_bytes=60 * 1024 * 1024
+        ),
+        name="experts",
+    )(heads, residual, norm_gain[None, :], route, out_weight, gate, up, down)
+
+
 def per_device(
     query_rows,
     key_rows,
@@ -238,44 +543,10 @@
     up_proj,
     down_proj,
 ):
-    tok_loc = residual.shape[0]
-    token_heads = mixer(query_rows, key_rows, value_rows, forget_cum, doc_ids)
-    mixed = jnp.dot(token_heads, out_weight, preferred_element_type=jnp.float32)
-    hidden = residual.astype(jnp.float32) + mixed
-    normed = (
-        hidden * lax.rsqrt(jnp.mean(hidden * hidden, axis=-1, keepdims=True) + norm_eps) * norm_gain
-    ).astype(jnp.bfloat16)
-    experts = lax.axis_size("sp")
-    groups = experts // EPG
-    capacity = max(2, 5 * tok_loc // (4 * groups))
-    width = normed.shape[1]
-    flat = expert_ids.reshape(-1)
-    onehot = (flat[:, None] == jnp.arange(experts, dtype=jnp.int32)[None, :]).astype(jnp.int32)
-    earlier = jnp.cumsum(onehot, axis=0) - onehot
-    slot_rank = jnp.sum(earlier * onehot, axis=1)
-    slot = flat * capacity + slot_rank
-    select = (jnp.arange(experts * capacity, dtype=jnp.int32)[:, None] == slot[None, :]).astype(
-        jnp.bfloat16
-    )
-    select_tokens = select.reshape(experts * capacity, tok_loc, TOPK).sum(axis=-1)
-    sent = jnp.dot(select_tokens, normed, preferred_element_type=jnp.float32).astype(jnp.bfloat16)
-    sent = sent.reshape(experts, capacity, width)
-    arrived = lax.all_to_all(sent, "sp", split_axis=0, concat_axis=0, tiled=True)
-    rows = arrived.reshape(-1, width)
-    gate = jnp.dot(rows, gate_proj[0], preferred_element_type=jnp.float32)
-    up = jnp.dot(rows, up_proj[0], preferred_element_type=jnp.float32)
-    act = (jax.nn.silu(gate) * up).astype(jnp.bfloat16)
-    outcome = jnp.dot(act, down_proj[0], preferred_element_type=jnp.float32).astype(jnp.bfloat16)
-    back = lax.all_to_all(
-        outcome.reshape(arrived.shape), "sp", split_axis=0, concat_axis=0, tiled=True
-    )
-    back_rows = back.reshape(experts * capacity, width)
-    picked = lax.dot_general(
-        select, back_rows, (((0,), (0,)), ((), ())), preferred_element_type=jnp.float32
-    )
-    picked = picked.reshape(tok_loc, TOPK, width)
-    combined = jnp.sum(picked * route_weights[:, :, None], axis=1)
-    return (hidden + combined).astype(jnp.bfloat16)
+    heads = mixer(query_rows, key_rows, value_rows, forget_cum, doc_ids)
+    return experts_layer(
+        heads, residual, out_weight, norm_gain, expert_ids, route_weights, gate_proj[0], up_proj[0], down_proj[0]
+    )
 
 
 def solution(mesh):

time: 282 us -> 178 us (0.63)
  the two profiles are of different devices: /device:TPU:2 before, /device:TPU:24 now
where the time goes in v2:
time: 178 us
  Pallas kernels  169 us (95%)
  local copies, waits for them, and re-layouts  5.58 us (3%)
  other arithmetic  3.48 us (2%)
    pallas_call x1, Pallas kernels, experts_layer(): pl.pallas_call(functools.partial(expert_kernel, capacity), out_shape=jax....  113 us
    pallas_call x1, Pallas kernels, mixer(): pl.pallas_call(functools.partial(mixer_kernel, n_sp, n_tp), out_shape=jax...  55.5 us
    unnamed x9, local copies, waits for them, and re-layouts  5.43 us

profile of v2, /device:TPU:24, one launch (start us, length us, event | category | flops | bytes accessed | tf_op | source)
XLA Modules:
  0.0 177.6 jit_solution(14860936259411363265)
XLA Ops:
  0.0 0.1 pad.2.clone
  0.1 0.1 pad.5.clone
  0.2 0.7 convert_bitcast_fusion
  0.8 1.3 maximum_maximum_fusion.1.route_ref
  2.2 0.7 convert_element_type.9
  2.9 0.8 maximum_maximum_fusion.marks_ref
  3.6 0.0 copy-start.1
  3.6 0.9 copy-done.1
  4.6 0.0 copy-start.2
  4.6 0.9 copy-done.2
  5.5 0.0 copy-start.3
  5.5 0.9 copy-done.3
  6.5 55.5 %mixer.1.heads_ref = bf16[128,1024]{1,0:T(8,128)(2,1)S(1)} custom-call(bf16[1024,128]{1,0:T(8,128)(2,1)S(1)} %copy-done.1, bf16[1024,128]{1,0:T(8,128)(2,1)S(1)} %copy-done.2, bf16[1024,128]{1,0:T(8,128)(2,1)S(1)} %copy-done.3, f32[8,1024]{1,0:T(8,128)S(1)} %maximum_maximum_fusion.marks_ref), custom_call_target="tpu_custom_call" | custom-call | tf_op jit(solution)/shard_map/mixer/pallas_call | solution.py:200
  62.0 0.0 copy-start
  62.0 0.7 copy-done
  62.7 113.0 %experts.1 = bf16[128,2048]{1,0:T(8,128)(2,1)} custom-call(bf16[128,1024]{1,0:T(8,128)(2,1)} %copy-done, bf16[128,2048]{1,0:T(8,128)(2,1)} %residual_ref.1, f32[1,2048]{1,0:T(1,128)} %bitcast.12, f32[8,128]{1,0:T(8,128)} %maximum_maximum_fusion.1.route_ref, bf16[1024,2048]{1,0:T(8,128)(2,1)} %mix_hbm.1, bf16[2048,512]{1,0:T(8,128)(2,1)} %bitcast.8, ...), custom_call_target="tpu_custom_call" | custom-call | tf_op jit(solution)/shard_map/experts/pallas_call | solution.py:501
  175.8 1.9 %copy.15 = bf16[128,2048]{1,0:T(8,128)(2,1)} copy(bf16[128,2048]{1,0:T(8,128)(2,1)} %experts.1) | data formatting | bytes 1048576
  (2 shorter events, 0.0 us)
Async XLA Ops:
  3.6 0.9 copy-start.1
  4.6 0.9 copy-start.2
  5.5 0.9 copy-start.3
  62.0 0.7 copy-start

commit v3 on v2

--- a/solution.py
+++ b/solution.py
@@ -9,9 +9,12 @@
 EPG = 4
 TOPK = 2
 REACH = 3
-QT = 256
+QT = 512
+QF = 1024
 KT = 512
 FAR = -1e30
+CUTS = 2
+STRAIGHT = ()
 
 norm_eps = 1e-06
 F32 = jnp.float32
@@ -24,37 +27,113 @@
 
 
 def mixer_kernel(
-    n_sp, n_tp, q_ref, k_ref, v_ref, marks_ref, out_ref,
-    kbuf, vbuf, mbuf, qaug, kmark, vaug, top, acc, att, heads,
-    ksend, krecv, vsend, vrecv, msend, mrecv, hsend, hrecv,
+    n_sp, n_tp, q_hbm, k_hbm, v_hbm, gate_ref, doc_ref, out_ref,
+    q_ref, k_ref, v_ref, marks_ref, krel, vrel, mrel,
+    kbuf, vbuf, mbuf, qaug, keyt, vaug, top, acc, att, heads,
+    load, rsend, rrecv, hsend, hrecv, asend, arecv,
 ):
     sp = lax.axis_index("sp")
     tp = lax.axis_index("tp")
     tok = q_ref.shape[0]
     chunk = tok // n_tp
 
+    x = lax.rem(sp, EPG)
+    z = sp // EPG
+    planes = n_sp // EPG
+
+    def along_x(hop):
+        return {"sp": z * EPG + lax.rem(x + hop, EPG)}
+
+    def along_z(hop):
+        return {"sp": lax.rem(z + hop, planes) * EPG + x}
+
     barrier = pltpu.get_barrier_semaphore()
+    for hop in range(1, EPG):
+        pl.semaphore_signal(barrier, inc=1, device_id=along_x(hop))
+    for hop in (1, planes - 1):
+        pl.semaphore_signal(barrier, inc=1, device_id=along_z(hop))
     for d in range(1, REACH + 1):
         for other in (lax.rem(sp + d, n_sp), lax.rem(sp + n_sp - d, n_sp)):
             pl.semaphore_signal(barrier, inc=1, device_id={"sp": other})
     for d in range(1, n_tp):
         pl.semaphore_signal(barrier, inc=1, device_id={"tp": lax.rem(tp + d, n_tp)})
-    pl.semaphore_wait(barrier, 2 * REACH + n_tp - 1)
-
-    halo = []
-    for d in range(1, REACH + 1):
-        ahead = {"sp": lax.rem(sp + d, n_sp)}
-        parts = []
-        for src, buf, send, recv in (
-            (marks_ref, mbuf, msend, mrecv), (k_ref, kbuf, ksend, krecv), (v_ref, vbuf, vsend, vrecv)
-        ):
-            copy = pltpu.make_async_remote_copy(
-                src_ref=src, dst_ref=buf.at[d - 1], send_sem=send.at[d - 1], recv_sem=recv.at[d - 1],
-                device_id=ahead,
-            )
-            copy.start()
-            parts.append(copy)
-        halo.append(parts)
+
+    loads = [
+        pltpu.make_async_copy(src, dst, load.at[i])
+        for i, (src, dst) in enumerate(((k_hbm, k_ref), (v_hbm, v_ref), (q_hbm, q_ref)))
+    ]
+    for copy in loads:
+        copy.start()
+    marks_ref[...] = jnp.concatenate(
+        [gate_ref[...], doc_ref[...].astype(F32), jnp.zeros((5, tok), F32)], axis=0
+    )
+    pl.semaphore_wait(barrier, EPG - 1 + 2 + 2 * REACH + n_tp - 1)
+
+    part = tok // CUTS
+    pieces = [(marks_ref, mrel, mbuf, None)]
+    for src, rel, buf in ((k_ref, krel, kbuf), (v_ref, vrel, vbuf)):
+        pieces += [(src, rel, buf, pl.ds(c * part, part)) for c in range(CUTS)]
+
+    def across(i):
+        src, rel, buf, rows = pieces[i]
+        if rows is not None:
+            src, rel = src.at[rows], rel.at[rows]
+        return pltpu.make_async_remote_copy(
+            src_ref=src, dst_ref=rel, send_sem=rsend.at[i], recv_sem=rrecv.at[i], device_id=along_z(1)
+        )
+
+    def along(i, d, relayed):
+        src, rel, buf, rows = pieces[i]
+        src = rel if relayed else src
+        dst = buf.at[d - 1]
+        if rows is not None:
+            src, dst = src.at[rows], dst.at[rows]
+        return pltpu.make_async_remote_copy(
+            src_ref=src, dst_ref=dst, send_sem=hsend.at[d - 1, i], recv_sem=hrecv.at[d - 1, i],
+            device_id=along_x(d) if relayed else {"sp": lax.rem(sp + d, n_sp)},
+        )
+
+    def straight(d):
+        here = x + d < EPG
+        for column, far in STRAIGHT:
+            if far == d:
+                here = here | (x == column)
+        return here
+
+    relays = sorted({c for c in range(1, EPG) for d in range(EPG - c, EPG) if (c, d) not in STRAIGHT})
+
+    def relaying():
+        here = x == relays[0]
+        for c in relays[1:]:
+            here = here | (x == c)
+        return here
+
+    for i in range(len(pieces)):
+        if i in (1, 1 + CUTS):
+            loads[0 if i == 1 else 1].wait()
+
+        @pl.when(relaying())
+        def _(i=i):
+            across(i).start()
+
+        for d in range(1, REACH + 1):
+
+            @pl.when(straight(d))
+            def _(i=i, d=d):
+                along(i, d, False).start()
+
+    loads[2].wait()
+
+    def pass_on(i):
+        @pl.when(relaying())
+        def _():
+            across(i).wait_recv()
+
+        for d in range(1, REACH + 1):
+
+            @pl.when(jnp.logical_not(straight(d)))
+            def _(d=d):
+                along(i, d, True).start()
 
     lane = lax.broadcasted_iota(jnp.int32, (1, 128), 1)
     row8 = lax.broadcasted_iota(jnp.int32, (8, tok), 0)
@@ -72,7 +151,7 @@
         qaug[h, :, 0:128] = jnp.where(mine, qrows, jnp.zeros_like(qrows))
         qaug[h, :, 128:256] = jnp.where(ones, jnp.ones_like(qmark), qmark)
 
-    def prepare(marks, v):
+    def prepare(marks, keys, v):
         gate = base - marks[0:2, :]
         high = gate.astype(BF16).astype(F32)
         rest = gate - high
@@ -83,23 +162,22 @@
             for i, piece in enumerate((high, mid, low)):
                 pieces = jnp.where(row8 == 3 * h + i, piece[h : h + 1, :], pieces)
         other = jnp.where(marks[2:3, :] == row16, 0.0, FAR).astype(F32)
-        kmark[...] = columns_of(jnp.concatenate([pieces, other, blank], axis=0))
+        keyt[128:256, :] = jnp.concatenate([pieces, other, blank], axis=0).astype(BF16)
+        for c in range(0, tok, 128):
+            keyt[0:128, c : c + 128] = jnp.transpose(keys[c : c + 128, :].astype(F32)).astype(BF16)
         one = jnp.ones_like(v)
         vaug[0] = jnp.where(lane < 64, v, one)
         vaug[1] = jnp.where(lane < 64, one, v)
 
-    def tile(keys, q0, k0, fresh, causal):
-        rows = pl.ds(q0, QT)
-        kk = jnp.concatenate([keys[pl.ds(k0, KT), :], kmark[pl.ds(k0, KT), :]], axis=1)
+    def tile(q0, k0, fresh, causal, wide=QT):
+        rows = pl.ds(q0, wide)
         for h in range(2):
-            score = lax.dot_general(
-                qaug[h, rows, :], kk, (((1,), (1,)), ((), ())), preferred_element_type=F32
-            )
+            score = jnp.dot(qaug[h, rows, :], keyt[:, pl.ds(k0, KT)], preferred_element_type=F32)
             if causal:
-                qpos = q0 + lax.broadcasted_iota(jnp.int32, (QT, KT), 0)
-                kpos = k0 + lax.broadcasted_iota(jnp.int32, (QT, KT), 1)
+                qpos = q0 + lax.broadcasted_iota(jnp.int32, (wide, KT), 0)
+                kpos = k0 + lax.broadcasted_iota(jnp.int32, (wide, KT), 1)
                 score = jnp.where(kpos <= qpos, score, FAR)
-            best = jnp.broadcast_to(jnp.max(score, axis=1, keepdims=True), (QT, 128))
+            best = jnp.broadcast_to(jnp.max(score, axis=1, keepdims=True), (wide, 128))
             if not fresh:
                 old = top[h, rows, :]
                 best = jnp.maximum(best, old)
@@ -110,44 +188,43 @@
             top[h, rows, :] = best
             acc[h, rows, :] = part
 
-    prepare(own, v_ref[...])
+    prepare(own, k_ref, v_ref[...])
     tiles = tok // QT
     per = KT // QT
     for k0 in range(0, tok, KT):
         first = k0 // QT
 
         def diagonal(i, carry, k0=k0):
-            tile(k_ref, pl.multiple_of(i * QT, QT), k0, k0 == 0, True)
+            tile(pl.multiple_of(i * QT, QT), k0, k0 == 0, True)
             return carry
 
         def below(i, carry, k0=k0):
-            tile(k_ref, pl.multiple_of(i * QT, QT), k0, k0 == 0, False)
+            tile(pl.multiple_of(i * QT, QT), k0, k0 == 0, False)
             return carry
 
         lax.fori_loop(first, first + per, diagonal, 0)
         if first + per < tiles:
             lax.fori_loop(first + per, tiles, below, 0)
 
+    for i in range(len(pieces)):
+        pass_on(i)
     for d in range(1, REACH + 1):
-        for copy in halo[d - 1]:
-            copy.wait_recv()
-        prepare(mbuf[d - 1], vbuf[d - 1])
-        keys = kbuf.at[d - 1]
+        for i in range(len(pieces)):
+            along(i, d, False).wait_recv()
+        prepare(mbuf[d - 1], kbuf.at[d - 1], vbuf[d - 1])
         if d < REACH:
 
-            def full(i, carry, keys=keys):
+            def full(i, carry):
                 for k0 in range(0, tok, KT):
-                    tile(keys, pl.multiple_of(i * QT, QT), k0, False, False)
+                    tile(pl.multiple_of(i * QF, QF), k0, False, False, QF)
                 return carry
 
-            lax.fori_loop(0, tiles, full, 0)
-
-    keys = kbuf.at[REACH - 1]
-    sends = []
+            lax.fori_loop(0, tok // QF, full, 0)
+
     for i in range(tiles):
         q0 = i * QT
         for k0 in range(q0 // KT * KT, tok, KT):
-            tile(keys, q0, k0, False, False)
+            tile(q0, k0, False, False)
         rows = pl.ds(q0, QT)
         total = jnp.where(lane < 64, pltpu.roll(acc[0, rows, :], 64, 1), pltpu.roll(acc[1, rows, :], 64, 1))
         value = jnp.where(lane < 64, acc[0, rows, :], acc[1, rows, :])
@@ -158,7 +235,7 @@
             def _(c=c):
                 pltpu.make_async_remote_copy(
                     src_ref=att.at[pl.ds(c * chunk, chunk)], dst_ref=heads.at[tp],
-                    send_sem=hsend.at[c], recv_sem=hrecv.at[tp], device_id={"tp": c},
+                    send_sem=asend.at[c], recv_sem=arecv.at[tp], device_id={"tp": c},
                 ).start()
 
     for c in range(n_tp):
@@ -167,7 +244,7 @@
         def _(c=c):
             pltpu.make_async_remote_copy(
                 src_ref=att.at[pl.ds(c * chunk, chunk)], dst_ref=heads.at[c],
-                send_sem=hsend.at[c], recv_sem=hrecv.at[c], device_id={"tp": c},
+                send_sem=asend.at[c], recv_sem=arecv.at[c], device_id={"tp": c},
             ).wait_recv()
             out_ref[:, c * 128 : (c + 1) * 128] = heads[c]
 
@@ -181,46 +258,58 @@
         def _(c=c):
             pltpu.make_async_remote_copy(
                 src_ref=att.at[pl.ds(c * chunk, chunk)], dst_ref=heads.at[c],
-                send_sem=hsend.at[c], recv_sem=hrecv.at[c], device_id={"tp": c},
+                send_sem=asend.at[c], recv_sem=arecv.at[c], device_id={"tp": c},
             ).wait_send()
 
-    for parts in halo:
-        for copy in parts:
-            copy.wait_send()
+    for i in range(len(pieces)):
+
+        @pl.when(relaying())
+        def _(i=i):
+            across(i).wait_send()
+
+        for d in range(1, REACH + 1):
+            along(i, d, False).wait_send()
 
 
 def mixer(query_rows, key_rows, value_rows, forget_cum, doc_ids):
     n_sp, n_tp = lax.axis_size("sp"), lax.axis_size("tp")
     tok, width = query_rows.shape
-    marks = jnp.concatenate(
-        [forget_cum, doc_ids.astype(F32)[None, :], jnp.zeros((5, tok), F32)], axis=0
-    )
     vmem = pl.BlockSpec(memory_space=pltpu.VMEM)
+    hbm = pl.BlockSpec(memory_space=pl.ANY)
     dma = pltpu.SemaphoreType.DMA
     return pl.pallas_call(
         functools.partial(mixer_kernel, n_sp, n_tp),
         out_shape=jax.ShapeDtypeStruct((tok // n_tp, width * n_tp), BF16),
-        in_specs=[vmem] * 4,
+        in_specs=[hbm] * 3 + [vmem] * 2,
         out_specs=vmem,
         scratch_shapes=[
+            pltpu.VMEM((tok, width), BF16),
+            pltpu.VMEM((tok, width), BF16),
+            pltpu.VMEM((tok, width), BF16),
+            pltpu.VMEM((8, tok), F32),
+            pltpu.VMEM((tok, width), BF16),
+            pltpu.VMEM((tok, width), BF16),
+            pltpu.VMEM((8, tok), F32),
             pltpu.VMEM((REACH, tok, width), BF16),
             pltpu.VMEM((REACH, tok, width), BF16),
             pltpu.VMEM((REACH, 8, tok), F32),
             pltpu.VMEM((2, tok, 2 * width), BF16),
-            pltpu.VMEM((tok, width), BF16),
+            pltpu.VMEM((2 * width, tok), BF16),
             pltpu.VMEM((2, tok, width), BF16),
             pltpu.VMEM((2, tok, 128), F32),
             pltpu.VMEM((2, tok, 128), F32),
             pltpu.VMEM((tok, width), BF16),
             pltpu.VMEM((n_tp, tok // n_tp, width), BF16),
-            dma((REACH,)), dma((REACH,)), dma((REACH,)), dma((REACH,)), dma((REACH,)), dma((REACH,)),
+            dma((3,)),
+            dma((1 + 2 * CUTS,)), dma((1 + 2 * CUTS,)),
+            dma((REACH, 1 + 2 * CUTS)), dma((REACH, 1 + 2 * CUTS)),
             dma((n_tp,)), dma((n_tp,)),
         ],
         compiler_params=pltpu.CompilerParams(
-            collective_id=0, has_side_effects=True, vmem_limit_bytes=48 * 1024 * 1024
+            collective_id=0, has_side_effects=True, vmem_limit_bytes=67043328
         ),
         name="mixer",
-    )(query_rows, key_rows, value_rows, marks)
+    )(query_rows, key_rows, value_rows, forget_cum, doc_ids[None, :])
 
 
 HOPS = (0, 1, 7, 2, 6, 3, 5, 4)
@@ -235,8 +324,8 @@
 
 
 def expert_kernel(
-    capacity, heads_ref, residual_ref, gain_ref, route_ref, mix_hbm, gate_hbm, up_hbm, down_hbm, out_ref,
-    mix, wgate, wup, wdown, hidden, normed, zs, zbuf, ms, mbuf, mcol, xs, xbuf, ys, ybuf, cs, cbuf,
+    capacity, heads_ref, gain_ref, ids_ref, weights_ref, residual_hbm, mix_hbm, gate_hbm, up_hbm, down_hbm, out_ref,
+    residual_ref, mix, wgate, wup, wdown, hidden, normed, zs, zbuf, ms, mbuf, mcol, xs, xbuf, ys, ybuf, cs, cbuf,
     load, zsend, zrecv, msend, mrecv, xsend, xrecv, ysend, yrecv, csend, crecv,
 ):
     sp = lax.axis_index("sp")
@@ -262,13 +351,13 @@
     loads = [
         pltpu.make_async_copy(src, dst, load.at[i])
         for i, (src, dst) in enumerate(
-            ((mix_hbm, mix), (gate_hbm, wgate), (up_hbm, wup), (down_hbm, wdown))
+            ((residual_hbm, residual_ref), (mix_hbm, mix), (gate_hbm, wgate), (up_hbm, wup), (down_hbm, wdown))
         )
     ]
     for copy in loads:
         copy.start()
 
-    ids = route_ref[0:2, :].astype(jnp.int32)
+    ids = ids_ref[...]
     id0, id1 = ids[0:1, :], ids[1:2, :]
     earlier = (
         lax.broadcasted_iota(jnp.int32, (tok, tok), 0) < lax.broadcasted_iota(jnp.int32, (tok, tok), 1)
@@ -283,8 +372,8 @@
         == lax.rem(x + lax.broadcasted_iota(jnp.int32, (16, planes * EPG), 0), EPG)
     ).astype(BF16)
     slots = jnp.dot(pick, (uses * (rank + 1.0)).astype(BF16), preferred_element_type=F32)
-    weight = jnp.where((id0 & (EPG - 1)) == which, route_ref[2:3, :], 0.0) + jnp.where(
-        (id1 & (EPG - 1)) == which, route_ref[3:4, :], 0.0
+    weight = jnp.where((id0 & (EPG - 1)) == which, weights_ref[0:1, :], 0.0) + jnp.where(
+        (id1 & (EPG - 1)) == which, weights_ref[1:2, :], 0.0
     )
     high = weight.astype(BF16).astype(F32)
     info = jnp.where(row < 4, slots, jnp.where(row < 8, high, jnp.where(row < 12, weight - high, 0.0)))
@@ -316,6 +405,7 @@
     cols = jnp.transpose(jnp.where(wide == 0, mine, jnp.where(wide == 1, place, 0.0)))
 
     loads[0].wait()
+    loads[1].wait()
     square = jnp.zeros((tok, 128), F32)
     for c in range(0, width, 512):
         part = jnp.dot(heads_ref[...], mix[:, c : c + 512], preferred_element_type=F32)
@@ -448,7 +538,7 @@
 
     spread(0)
     spread(1)
-    for copy in loads[1:]:
+    for copy in loads[2:]:
         copy.wait()
     expert(0)
     spread(2)
@@ -490,9 +580,6 @@
     planes = lax.axis_size("sp") // EPG
     capacity = max(2, 5 * tok // (4 * planes))
     group = 2 * capacity
-    route = jnp.concatenate(
-        [expert_ids.T.astype(F32), route_weights.T, jnp.zeros((4, tok), F32)], axis=0
-    )
     vmem = pl.BlockSpec(memory_space=pltpu.VMEM)
     hbm = pl.BlockSpec(memory_space=pl.ANY)
     dma = pltpu.SemaphoreType.DMA
@@ -501,9 +588,10 @@
     return pl.pallas_call(
         functools.partial(expert_kernel, capacity),
         out_shape=jax.ShapeDtypeStruct((tok, width), BF16),
-        in_specs=[vmem] * 4 + [hbm] * 4,
+        in_specs=[vmem] * 4 + [hbm] * 5,
         out_specs=vmem,
         scratch_shapes=[
+            pltpu.VMEM((tok, width), BF16),
             pltpu.VMEM(out_weight.shape, BF16),
             pltpu.VMEM(gate.shape, BF16),
             pltpu.VMEM(up.shape, BF16),
@@ -516,16 +604,16 @@
             pltpu.VMEM((planes, group, 128), F32),
             quads, quads, quads, quads,
             slots, slots,
-            dma((4,)),
+            dma((5,)),
             dma((planes,)), dma((planes,)), dma((planes,)), dma((planes,)),
             dma((PAIRS, EPG)), dma((PAIRS, EPG)), dma((PAIRS, EPG)), dma((PAIRS, EPG)),
             dma((planes,)), dma((planes,)),
         ],
         compiler_params=pltpu.CompilerParams(
-            collective_id=1, has_side_effects=True, vmem_limit_bytes=60 * 1024 * 1024
+            collective_id=1, has_side_effects=True, vmem_limit_bytes=67043328
         ),
         name="experts",
-    )(heads, residual, norm_gain[None, :], route, out_weight, gate, up, down)
+    )(heads, norm_gain[None, :], expert_ids.T, route_weights.T, residual, out_weight, gate, up, down)
 
 
 def per_device(

time: 178 us -> 150 us (0.84)
  the two profiles are of different devices: /device:TPU:24 before, /device:TPU:2 now
where the time goes in v3:
time: 150 us; the launch traced here: 147 us
  Pallas kernels  145 us (97%)
  local copies, waits for them, and re-layouts  1.88 us (1%)
    pallas_call x1, Pallas kernels, experts_layer(): pl.pallas_call(functools.partial(expert_kernel, capacity), out_shape=jax....  97.2 us
    pallas_call x1, Pallas kernels, mixer(): pl.pallas_call(functools.partial(mixer_kernel, n_sp, n_tp), out_shape=jax...  47.9 us

profile of v3, /device:TPU:2, one launch (start us, length us, event | category | flops | bytes accessed | tf_op | source)
XLA Modules:
  0.0 147.0 jit_solution(9899810784162267344)
XLA Ops:
  0.0 47.9 %mixer.1.heads_ref = bf16[128,1024]{1,0:T(8,128)(2,1)} custom-call(bf16[1024,128]{1,0:T(8,128)(2,1)} %q_hbm.1, bf16[1024,128]{1,0:T(8,128)(2,1)} %k_hbm.1, bf16[1024,128]{1,0:T(8,128)(2,1)} %v_hbm.1, f32[2,1024]{1,0:T(2,128)} %gate_ref.1, s32[1,1024]{1,0:T(1,128)} %bitcast.11), custom_call_target="tpu_custom_call" | custom-call | tf_op jit(solution)/shard_map/mixer/pallas_call | solution.py:280
  47.9 97.2 %experts.1 = bf16[128,2048]{1,0:T(8,128)(2,1)} custom-call(bf16[128,1024]{1,0:T(8,128)(2,1)} %mixer.1.heads_ref, f32[1,2048]{1,0:T(1,128)} %bitcast.10, s32[2,128]{1,0:T(2,128)} %bitcast.12, f32[2,128]{1,0:T(2,128)} %bitcast.13, bf16[128,2048]{1,0:T(8,128)(2,1)} %residual_hbm.1, bf16[1024,2048]{1,0:T(8,128)(2,1)} %mix_hbm.1, bf16[2048,512]{1,0:T(8,128)(2,1)} %bitcast.7, ...), custom_call_target="tpu_custom_call" | custom-call | tf_op jit(solution)/shard_map/experts/pallas_call | solution.py:588
  145.1 1.9 %copy.15 = bf16[128,2048]{1,0:T(8,128)(2,1)} copy(bf16[128,2048]{1,0:T(8,128)(2,1)} %experts.1) | data formatting | bytes 1048576

commit v4 on v3

--- a/solution.py
+++ b/solution.py
@@ -312,8 +312,10 @@
     )(query_rows, key_rows, value_rows, forget_cum, doc_ids[None, :])
 
 
-HOPS = (0, 1, 7, 2, 6, 3, 5, 4)
+HOPS = (2, 6, 3, 5, 4, 0, 1, 7)
 PAIRS = len(HOPS) // 2
+HERE = HOPS.index(0)
+AWAY = [s for s in range(len(HOPS)) if s != HERE]
 
 
 def stack(blocks):
@@ -396,8 +398,8 @@
         rest = jnp.zeros((16, 64 - group), F32)
         table = [table, rest, jnp.zeros((16, 64), F32)] if s % 2 == 0 else [jnp.zeros((16, 64), F32), table, rest]
         table = jnp.concatenate(table, axis=1)
-        if s == 0:
-            mbuf[0] = table
+        if s == HERE:
+            mbuf[s] = table
         else:
             ms[s] = table
     sel = jnp.concatenate(sel, axis=0).astype(BF16)
@@ -421,9 +423,9 @@
 
     for c in range(0, width, 512):
         part = jnp.dot(sel, normed[:, c : c + 512], preferred_element_type=F32)
-        zbuf[0, :, c : c + 512] = part[0:group].astype(BF16)
-        for s in range(1, planes):
-            zs[s, :, c : c + 512] = part[s * group : (s + 1) * group].astype(BF16)
+        for s in range(planes):
+            into = zbuf if s == HERE else zs
+            into[s, :, c : c + 512] = part[s * group : (s + 1) * group].astype(BF16)
     pl.semaphore_wait(barrier, planes + EPG - 2)
 
     def zcopy(s):
@@ -456,14 +458,14 @@
             device_id=along_z(planes - HOPS[s]),
         )
 
-    for s in range(1, planes):
+    for s in AWAY:
         mcopy(s).start()
         zcopy(s).start()
 
     def spread(p):
         for half in range(2):
             s = 2 * p + half
-            if s:
+            if s != HERE:
                 mcopy(s).wait_recv()
             table = jnp.concatenate([mbuf[s], jnp.zeros((112, 128), F32)], axis=0)
             mcol[s] = jnp.transpose(table)[64 * half : 64 * half + group, :]
@@ -473,7 +475,7 @@
         rows = [jnp.where(table[h : h + 1, :] == want, 1.0, 0.0) for h in range(EPG)]
         order = jnp.concatenate(rows, axis=0).astype(BF16)
         for half in range(2):
-            if 2 * p + half:
+            if 2 * p + half != HERE:
                 zcopy(2 * p + half).wait_recv()
         for c in range(0, width, 512):
             rows = stack([zbuf[2 * p, :, c : c + 512], zbuf[2 * p + 1, :, c : c + 512]])
@@ -528,28 +530,27 @@
             for half in range(2):
                 both = part[half * group : (half + 1) * group] + part[(2 + half) * group : (3 + half) * group]
                 s = 2 * p + half
-                if s:
-                    cs[s, :, c : c + 512] = both.astype(BF16)
-                else:
-                    cbuf[0, :, c : c + 512] = both.astype(BF16)
+                into = cbuf if s == HERE else cs
+                into[s, :, c : c + 512] = both.astype(BF16)
         for half in range(2):
-            if 2 * p + half:
+            if 2 * p + half != HERE:
                 ccopy(2 * p + half).start()
 
     spread(0)
-    spread(1)
     for copy in loads[2:]:
         copy.wait()
     expert(0)
+    spread(1)
+    collect(0)
+    expert(1)
     spread(2)
-    expert(1)
-    collect(0)
     spread(3)
+    collect(1)
     expert(2)
-    collect(1)
     expert(3)
     collect(2)
     collect(3)
+
     lanes = lax.broadcasted_iota(jnp.int32, (tok, 128), 1)
     back = []
     for p in range(PAIRS):
@@ -557,14 +558,14 @@
         hit = (cols[:, 0:1] == there.astype(F32)) & (cols[:, 1:2] == (lanes & 63).astype(F32))
         back.append(jnp.where(hit, 1.0, 0.0))
     back = jnp.concatenate(back, axis=1).astype(BF16)
-    for s in range(1, planes):
+    for s in AWAY:
         ccopy(s).wait_recv()
     for c in range(0, width, 512):
         rows = stack([cbuf[s, :, c : c + 512] for s in range(planes)])
         part = jnp.dot(back, rows, preferred_element_type=F32)
-        out_ref[:, c : c + 512] = (hidden[:, c : c + 512] + part).astype(BF16)
-
-    for s in range(1, planes):
+        out_ref[:, c : c + 512] = hidden[:, c : c + 512] + part
+
+    for s in AWAY:
         mcopy(s).wait_send()
         zcopy(s).wait_send()
         ccopy(s).wait_send()
@@ -587,7 +588,7 @@
     quads = pltpu.VMEM((PAIRS, EPG, group, width), BF16)
     return pl.pallas_call(
         functools.partial(expert_kernel, capacity),
-        out_shape=jax.ShapeDtypeStruct((tok, width), BF16),
+        out_shape=jax.ShapeDtypeStruct((tok, width), F32),
         in_specs=[vmem] * 4 + [hbm] * 5,
         out_specs=vmem,
         scratch_shapes=[
@@ -613,7 +614,7 @@
             collective_id=1, has_side_effects=True, vmem_limit_bytes=67043328
         ),
         name="experts",
-    )(heads, norm_gain[None, :], expert_ids.T, route_weights.T, residual, out_weight, gate, up, down)
+    )(heads, norm_gain[None, :], expert_ids.T, route_weights.T, residual, out_weight, gate, up, down).astype(BF16)
 
 
 def per_device(

time: 150 us -> 144 us (0.960); the launches traced: 147 us -> 143 us
  Pallas kernels: 145 us -> 140 us
  other arithmetic: 0 us -> 2.09 us
  local copies, waits for them, and re-layouts: 1.88 us -> 0 us
    pallas_call x1, Pallas kernels: 97.2 us -> 92.6 us  [experts_layer(): pl.pallas_call(functools.partial(expert_kernel, capacity), out_shape=jax....]
    convert_element_type x0 -> x1, other arithmetic: none -> 2.09 us  [experts_layer(): return pl.pallas_call(functools.partial(expert_kernel, capacity), out_sha...]
    unnamed x1 -> x0, local copies, waits for them, and re-layouts: 1.88 us -> none
where the time goes in v4:
time: 144 us; the launch traced here: 143 us
  Pallas kernels  140 us (97%)
  other arithmetic  2.09 us (1%)
    pallas_call x1, Pallas kernels, experts_layer(): pl.pallas_call(functools.partial(expert_kernel, capacity), out_shape=jax....  92.6 us
    pallas_call x1, Pallas kernels, mixer(): pl.pallas_call(functools.partial(mixer_kernel, n_sp, n_tp), out_shape=jax...  47.9 us

profile of v4, /device:TPU:2, one launch (start us, length us, event | category | flops | bytes accessed | tf_op | source)
XLA Modules:
  0.0 142.6 jit_solution(17015013368892440315)
XLA Ops:
  0.0 47.9 %mixer.1.heads_ref = bf16[128,1024]{1,0:T(8,128)(2,1)} custom-call(bf16[1024,128]{1,0:T(8,128)(2,1)} %q_hbm.1, bf16[1024,128]{1,0:T(8,128)(2,1)} %k_hbm.1, bf16[1024,128]{1,0:T(8,128)(2,1)} %v_hbm.1, f32[2,1024]{1,0:T(2,128)} %gate_ref.1, s32[1,1024]{1,0:T(1,128)} %bitcast.11), custom_call_target="tpu_custom_call" | custom-call | tf_op jit(solution)/shard_map/mixer/pallas_call | solution.py:280
  47.9 92.6 %experts.1 = f32[128,2048]{1,0:T(8,128)} custom-call(bf16[128,1024]{1,0:T(8,128)(2,1)} %mixer.1.heads_ref, f32[1,2048]{1,0:T(1,128)} %bitcast.10, s32[2,128]{1,0:T(2,128)} %bitcast.12, f32[2,128]{1,0:T(2,128)} %bitcast.13, bf16[128,2048]{1,0:T(8,128)(2,1)} %residual_hbm.1, bf16[1024,2048]{1,0:T(8,128)(2,1)} %mix_hbm.1, bf16[2048,512]{1,0:T(8,128)(2,1)} %bitcast.7, ...), custom_call_target="tpu_custom_call" | custom-call | tf_op jit(solution)/shard_map/experts/pallas_call | solution.py:589
  140.5 2.1 %convert_element_type.3 = bf16[128,2048]{1,0:T(8,128)(2,1)} convert(f32[128,2048]{1,0:T(8,128)} %experts.1) | non-fusion elementwise | flops 262144 | bytes 1572864 | tf_op jit(solution)/shard_map/convert_element_type | solution.py:617

commit v5 on v4

--- a/solution.py
+++ b/solution.py
@@ -14,7 +14,6 @@
 KT = 512
 FAR = -1e30
 CUTS = 2
-STRAIGHT = ()
 
 norm_eps = 1e-06
 F32 = jnp.float32
@@ -26,8 +25,8 @@
     return jnp.concatenate(parts, axis=0).astype(BF16)
 
 
-def mixer_kernel(
-    n_sp, n_tp, q_hbm, k_hbm, v_hbm, gate_ref, doc_ref, out_ref,
+def mix_heads(
+    n_sp, n_tp, early, q_hbm, k_hbm, v_hbm, gate_ref, doc_ref, out_ref,
     q_ref, k_ref, v_ref, marks_ref, krel, vrel, mrel,
     kbuf, vbuf, mbuf, qaug, keyt, vaug, top, acc, att, heads,
     load, rsend, rrecv, hsend, hrecv, asend, arecv,
@@ -50,11 +49,8 @@
     barrier = pltpu.get_barrier_semaphore()
     for hop in range(1, EPG):
         pl.semaphore_signal(barrier, inc=1, device_id=along_x(hop))
-    for hop in (1, planes - 1):
+    for hop in range(1, planes):
         pl.semaphore_signal(barrier, inc=1, device_id=along_z(hop))
-    for d in range(1, REACH + 1):
-        for other in (lax.rem(sp + d, n_sp), lax.rem(sp + n_sp - d, n_sp)):
-            pl.semaphore_signal(barrier, inc=1, device_id={"sp": other})
     for d in range(1, n_tp):
         pl.semaphore_signal(barrier, inc=1, device_id={"tp": lax.rem(tp + d, n_tp)})
 
@@ -67,7 +63,7 @@
     marks_ref[...] = jnp.concatenate(
         [gate_ref[...], doc_ref[...].astype(F32), jnp.zeros((5, tok), F32)], axis=0
     )
-    pl.semaphore_wait(barrier, EPG - 1 + 2 + 2 * REACH + n_tp - 1)
+    pl.semaphore_wait(barrier, EPG + planes - 2 + n_tp - 1)
 
     part = tok // CUTS
     pieces = [(marks_ref, mrel, mbuf, None)]
@@ -90,48 +86,33 @@
             src, dst = src.at[rows], dst.at[rows]
         return pltpu.make_async_remote_copy(
             src_ref=src, dst_ref=dst, send_sem=hsend.at[d - 1, i], recv_sem=hrecv.at[d - 1, i],
-            device_id=along_x(d) if relayed else {"sp": lax.rem(sp + d, n_sp)},
-        )
-
-    def straight(d):
-        here = x + d < EPG
-        for column, far in STRAIGHT:
-            if far == d:
-                here = here | (x == column)
-        return here
-
-    relays = sorted({c for c in range(1, EPG) for d in range(EPG - c, EPG) if (c, d) not in STRAIGHT})
-
-    def relaying():
-        here = x == relays[0]
-        for c in relays[1:]:
-            here = here | (x == c)
-        return here
+            device_id=along_x(d),
+        )
 
     for i in range(len(pieces)):
         if i in (1, 1 + CUTS):
             loads[0 if i == 1 else 1].wait()
 
-        @pl.when(relaying())
+        @pl.when(x > 0)
         def _(i=i):
             across(i).start()
 
         for d in range(1, REACH + 1):
 
-            @pl.when(straight(d))
+            @pl.when(x + d < EPG)
             def _(i=i, d=d):
                 along(i, d, False).start()
 
     loads[2].wait()
 
     def pass_on(i):
-        @pl.when(relaying())
+        @pl.when(x > 0)
         def _():
             across(i).wait_recv()
 
         for d in range(1, REACH + 1):
 
-            @pl.when(jnp.logical_not(straight(d)))
+            @pl.when(x + d >= EPG)
             def _(d=d):
                 along(i, d, True).start()
 
@@ -206,6 +187,7 @@
         if first + per < tiles:
             lax.fori_loop(first + per, tiles, below, 0)
 
+    early()
     for i in range(len(pieces)):
         pass_on(i)
     for d in range(1, REACH + 1):
@@ -252,64 +234,26 @@
         def _(c=c):
             out_ref[:, c * 128 : (c + 1) * 128] = att[c * chunk : (c + 1) * chunk, :]
 
-    for c in range(n_tp):
-
-        @pl.when(tp != c)
-        def _(c=c):
-            pltpu.make_async_remote_copy(
-                src_ref=att.at[pl.ds(c * chunk, chunk)], dst_ref=heads.at[c],
-                send_sem=asend.at[c], recv_sem=arecv.at[c], device_id={"tp": c},
-            ).wait_send()
-
-    for i in range(len(pieces)):
-
-        @pl.when(relaying())
-        def _(i=i):
-            across(i).wait_send()
-
-        for d in range(1, REACH + 1):
-            along(i, d, False).wait_send()
-
-
-def mixer(query_rows, key_rows, value_rows, forget_cum, doc_ids):
-    n_sp, n_tp = lax.axis_size("sp"), lax.axis_size("tp")
-    tok, width = query_rows.shape
-    vmem = pl.BlockSpec(memory_space=pltpu.VMEM)
-    hbm = pl.BlockSpec(memory_space=pl.ANY)
-    dma = pltpu.SemaphoreType.DMA
-    return pl.pallas_call(
-        functools.partial(mixer_kernel, n_sp, n_tp),
-        out_shape=jax.ShapeDtypeStruct((tok // n_tp, width * n_tp), BF16),
-        in_specs=[hbm] * 3 + [vmem] * 2,
-        out_specs=vmem,
-        scratch_shapes=[
-            pltpu.VMEM((tok, width), BF16),
-            pltpu.VMEM((tok, width), BF16),
-            pltpu.VMEM((tok, width), BF16),
-            pltpu.VMEM((8, tok), F32),
-            pltpu.VMEM((tok, width), BF16),
-            pltpu.VMEM((tok, width), BF16),
-            pltpu.VMEM((8, tok), F32),
-            pltpu.VMEM((REACH, tok, width), BF16),
-            pltpu.VMEM((REACH, tok, width), BF16),
-            pltpu.VMEM((REACH, 8, tok), F32),
-            pltpu.VMEM((2, tok, 2 * width), BF16),
-            pltpu.VMEM((2 * width, tok), BF16),
-            pltpu.VMEM((2, tok, width), BF16),
-            pltpu.VMEM((2, tok, 128), F32),
-            pltpu.VMEM((2, tok, 128), F32),
-            pltpu.VMEM((tok, width), BF16),
-            pltpu.VMEM((n_tp, tok // n_tp, width), BF16),
-            dma((3,)),
-            dma((1 + 2 * CUTS,)), dma((1 + 2 * CUTS,)),
-            dma((REACH, 1 + 2 * CUTS)), dma((REACH, 1 + 2 * CUTS)),
-            dma((n_tp,)), dma((n_tp,)),
-        ],
-        compiler_params=pltpu.CompilerParams(
-            collective_id=0, has_side_effects=True, vmem_limit_bytes=67043328
-        ),
-        name="mixer",
-    )(query_rows, key_rows, value_rows, forget_cum, doc_ids[None, :])
+    def drain():
+        for c in range(n_tp):
+
+            @pl.when(tp != c)
+            def _(c=c):
+                pltpu.make_async_remote_copy(
+                    src_ref=att.at[pl.ds(c * chunk, chunk)], dst_ref=heads.at[c],
+                    send_sem=asend.at[c], recv_sem=arecv.at[c], device_id={"tp": c},
+                ).wait_send()
+
+        for i in range(len(pieces)):
+
+            @pl.when(x > 0)
+            def _(i=i):
+                across(i).wait_send()
+
+            for d in range(1, REACH + 1):
+                along(i, d, False).wait_send()
+
+    return drain
 
 
 HOPS = (2, 6, 3, 5, 4, 0, 1, 7)
@@ -325,7 +269,7 @@
     return jnp.concatenate(parts, axis=0).astype(BF16)
 
 
-def expert_kernel(
+def route_and_run(
     capacity, heads_ref, gain_ref, ids_ref, weights_ref, residual_hbm, mix_hbm, gate_hbm, up_hbm, down_hbm, out_ref,
     residual_ref, mix, wgate, wup, wdown, hidden, normed, zs, zbuf, ms, mbuf, mcol, xs, xbuf, ys, ybuf, cs, cbuf,
     load, zsend, zrecv, msend, mrecv, xsend, xrecv, ysend, yrecv, csend, crecv,
@@ -343,12 +287,6 @@
 
     def along_x(hop):
         return {"sp": z * EPG + lax.rem(x + hop, EPG)}
-
-    barrier = pltpu.get_barrier_semaphore()
-    for hop in range(1, planes):
-        pl.semaphore_signal(barrier, inc=1, device_id=along_z(hop))
-    for hop in range(1, EPG):
-        pl.semaphore_signal(barrier, inc=1, device_id=along_x(hop))
 
     loads = [
         pltpu.make_async_copy(src, dst, load.at[i])
@@ -406,6 +344,8 @@
     wide = lax.broadcasted_iota(jnp.int32, (tok, tok), 0)
     cols = jnp.transpose(jnp.where(wide == 0, mine, jnp.where(wide == 1, place, 0.0)))
 
+    yield
+
     loads[0].wait()
     loads[1].wait()
     square = jnp.zeros((tok, 128), F32)
@@ -426,7 +366,6 @@
         for s in range(planes):
             into = zbuf if s == HERE else zs
             into[s, :, c : c + 512] = part[s * group : (s + 1) * group].astype(BF16)
-    pl.semaphore_wait(barrier, planes + EPG - 2)
 
     def zcopy(s):
         return pltpu.make_async_remote_copy(
@@ -563,7 +502,7 @@
     for c in range(0, width, 512):
         rows = stack([cbuf[s, :, c : c + 512] for s in range(planes)])
         part = jnp.dot(back, rows, preferred_element_type=F32)
-        out_ref[:, c : c + 512] = hidden[:, c : c + 512] + part
+        out_ref[:, c : c + 512] = (hidden[:, c : c + 512] + part).astype(BF16)
 
     for s in AWAY:
         mcopy(s).wait_send()
@@ -575,10 +514,26 @@
             ycopy(p, h).wait_send()
 
 
-def experts_layer(heads, residual, out_weight, norm_gain, expert_ids, route_weights, gate, up, down):
+def layer_kernel(n_sp, n_tp, capacity, parts, *refs):
+    cuts = [sum(parts[:i]) for i in range(len(parts) + 1)]
+    mixed_in, later_in, out, joined, mixer_scratch, later_scratch = (
+        refs[a:b] for a, b in zip(cuts, cuts[1:])
+    )
+    later = route_and_run(capacity, *joined, *later_in, *out, *later_scratch)
+    drain = mix_heads(n_sp, n_tp, lambda: next(later), *mixed_in, *joined, *mixer_scratch)
+    for _ in later:
+        pass
+    drain()
+
+
+def layer(
+    query_rows, key_rows, value_rows, forget_cum, doc_ids, residual, out_weight, norm_gain, expert_ids,
+    route_weights, gate, up, down,
+):
+    n_sp, n_tp = lax.axis_size("sp"), lax.axis_size("tp")
+    span, heads = query_rows.shape
     tok, width = residual.shape
-    ffe = gate.shape[1]
-    planes = lax.axis_size("sp") // EPG
+    planes = n_sp // EPG
     capacity = max(2, 5 * tok // (4 * planes))
     group = 2 * capacity
     vmem = pl.BlockSpec(memory_space=pltpu.VMEM)
@@ -586,35 +541,63 @@
     dma = pltpu.SemaphoreType.DMA
     slots = pltpu.VMEM((planes, group, width), BF16)
     quads = pltpu.VMEM((PAIRS, EPG, group, width), BF16)
+    mixer_scratch = [
+        pltpu.VMEM((span, heads), BF16),
+        pltpu.VMEM((span, heads), BF16),
+        pltpu.VMEM((span, heads), BF16),
+        pltpu.VMEM((8, span), F32),
+        pltpu.VMEM((span, heads), BF16),
+        pltpu.VMEM((span, heads), BF16),
+        pltpu.VMEM((8, span), F32),
+        pltpu.VMEM((REACH, span, heads), BF16),
+        pltpu.VMEM((REACH, span, heads), BF16),
+        pltpu.VMEM((REACH, 8, span), F32),
+        pltpu.VMEM((2, span, 2 * heads), BF16),
+        pltpu.VMEM((2 * heads, span), BF16),
+        pltpu.VMEM((2, span, heads), BF16),
+        pltpu.VMEM((2, span, 128), F32),
+        pltpu.VMEM((2, span, 128), F32),
+        pltpu.VMEM((span, heads), BF16),
+        pltpu.VMEM((n_tp, tok, heads), BF16),
+        dma((3,)),
+        dma((1 + 2 * CUTS,)), dma((1 + 2 * CUTS,)),
+        dma((REACH, 1 + 2 * CUTS)), dma((REACH, 1 + 2 * CUTS)),
+        dma((n_tp,)), dma((n_tp,)),
+    ]
+    later_scratch = [
+        pltpu.VMEM((tok, width), BF16),
+        pltpu.VMEM(out_weight.shape, BF16),
+        pltpu.VMEM(gate.shape, BF16),
+        pltpu.VMEM(up.shape, BF16),
+        pltpu.VMEM(down.shape, BF16),
+        pltpu.VMEM((tok, width), F32),
+        pltpu.VMEM((tok, width), BF16),
+        slots, slots,
+        pltpu.VMEM((planes, 16, 128), F32),
+        pltpu.VMEM((planes, 16, 128), F32),
+        pltpu.VMEM((planes, group, 128), F32),
+        quads, quads, quads, quads,
+        slots, slots,
+        dma((5,)),
+        dma((planes,)), dma((planes,)), dma((planes,)), dma((planes,)),
+        dma((PAIRS, EPG)), dma((PAIRS, EPG)), dma((PAIRS, EPG)), dma((PAIRS, EPG)),
+        dma((planes,)), dma((planes,)),
+    ]
+    parts = (5, 8, 1, 1, len(mixer_scratch), len(later_scratch))
     return pl.pallas_call(
-        functools.partial(expert_kernel, capacity),
-        out_shape=jax.ShapeDtypeStruct((tok, width), F32),
-        in_specs=[vmem] * 4 + [hbm] * 5,
+        functools.partial(layer_kernel, n_sp, n_tp, capacity, parts),
+        out_shape=jax.ShapeDtypeStruct((tok, width), BF16),
+        in_specs=[hbm] * 3 + [vmem] * 5 + [hbm] * 5,
         out_specs=vmem,
-        scratch_shapes=[
-            pltpu.VMEM((tok, width), BF16),
-            pltpu.VMEM(out_weight.shape, BF16),
-            pltpu.VMEM(gate.shape, BF16),
-            pltpu.VMEM(up.shape, BF16),
-            pltpu.VMEM(down.shape, BF16),
-            pltpu.VMEM((tok, width), F32),
-            pltpu.VMEM((tok, width), BF16),
-            slots, slots,
-            pltpu.VMEM((planes, 16, 128), F32),
-            pltpu.VMEM((planes, 16, 128), F32),
-            pltpu.VMEM((planes, group, 128), F32),
-            quads, quads, quads, quads,
-            slots, slots,
-            dma((5,)),
-            dma((planes,)), dma((planes,)), dma((planes,)), dma((planes,)),
-            dma((PAIRS, EPG)), dma((PAIRS, EPG)), dma((PAIRS, EPG)), dma((PAIRS, EPG)),
-            dma((planes,)), dma((planes,)),
-        ],
+        scratch_shapes=[pltpu.VMEM((tok, heads * n_tp), BF16)] + mixer_scratch + later_scratch,
         compiler_params=pltpu.CompilerParams(
-            collective_id=1, has_side_effects=True, vmem_limit_bytes=67043328
+            collective_id=0, has_side_effects=True, vmem_limit_bytes=67043328
         ),
-        name="experts",
-    )(heads, norm_gain[None, :], expert_ids.T, route_weights.T, residual, out_weight, gate, up, down).astype(BF16)
+        name="layer",
+    )(
+        query_rows, key_rows, value_rows, forget_cum, doc_ids[None, :], norm_gain[None, :], expert_ids.T,
+        route_weights.T, residual, out_weight, gate, up, down,
+    )
 
 
 def per_device(
@@ -632,9 +615,9 @@
     up_proj,
     down_proj,
 ):
-    heads = mixer(query_rows, key_rows, value_rows, forget_cum, doc_ids)
-    return experts_layer(
-        heads, residual, out_weight, norm_gain, expert_ids, route_weights, gate_proj[0], up_proj[0], down_proj[0]
+    return layer(
+        query_rows, key_rows, value_rows, forget_cum, doc_ids, residual, out_weight, norm_gain, expert_ids,
+        route_weights, gate_proj[0], up_proj[0], down_proj[0],
     )
 
 

time: 144 us -> 141 us (0.979)
  other arithmetic: 2.09 us -> 0 us
  local copies, waits for them, and re-layouts: 0 us -> 1.88 us
    convert_element_type x1 -> x0, other arithmetic: 2.09 us -> none  [experts_layer(): return pl.pallas_call(functools.partial(expert_kernel, capacity), out_sha...]
    unnamed x0 -> x1, local copies, waits for them, and re-layouts: none -> 1.88 us
    pallas_call x2 -> x1, Pallas kernels: 140 us -> 139 us  [layer(): pl.pallas_call(functools.partial(layer_kernel, n_sp, n_tp, capacity, part...]
where the time goes in v5:
time: 141 us
  Pallas kernels  139 us (99%)
  local copies, waits for them, and re-layouts  1.88 us (1%)
    pallas_call x1, Pallas kernels, layer(): pl.pallas_call(functools.partial(layer_kernel, n_sp, n_tp, capacity, part...  139 us

profile of v5, /device:TPU:2, one launch (start us, length us, event | category | flops | bytes accessed | tf_op | source)
XLA Modules:
  0.0 140.8 jit_solution(6132812212791072704)
XLA Ops:
  0.0 138.9 %layer.1 = bf16[128,2048]{1,0:T(8,128)(2,1)} custom-call(bf16[1024,128]{1,0:T(8,128)(2,1)} %refs_0_.1, bf16[1024,128]{1,0:T(8,128)(2,1)} %refs_1_.1, bf16[1024,128]{1,0:T(8,128)(2,1)} %refs_2_.1, f32[2,1024]{1,0:T(2,128)} %refs_3_.1, s32[1,1024]{1,0:T(1,128)} %bitcast.11, f32[1,2048]{1,0:T(1,128)} %bitcast.10, s32[2,128]{1,0:T(2,128)} %bitcast.12, ...), custom_call_target="tpu_custom_call" | custom-call | tf_op jit(solution)/shard_map/layer/pallas_call | solution.py:587
  138.9 1.9 %copy.15 = bf16[128,2048]{1,0:T(8,128)(2,1)} copy(bf16[128,2048]{1,0:T(8,128)(2,1)} %layer.1) | data formatting | bytes 1048576

commit v6 on v5

--- a/solution.py
+++ b/solution.py
@@ -29,7 +29,7 @@
     n_sp, n_tp, early, q_hbm, k_hbm, v_hbm, gate_ref, doc_ref, out_ref,
     q_ref, k_ref, v_ref, marks_ref, krel, vrel, mrel,
     kbuf, vbuf, mbuf, qaug, keyt, vaug, top, acc, att, heads,
-    load, rsend, rrecv, hsend, hrecv, asend, arecv,
+    load, fsend, rsend, rrecv, hsend, hrecv, asend, arecv,
 ):
     sp = lax.axis_index("sp")
     tp = lax.axis_index("tp")
@@ -110,11 +110,22 @@
         def _():
             across(i).wait_recv()
 
-        for d in range(1, REACH + 1):
+        for d in (1, 3):
 
             @pl.when(x + d >= EPG)
             def _(d=d):
                 along(i, d, True).start()
+
+    handing = (x == 1) | (x == 2)
+
+    def hand_on(i):
+        buf, rows = pieces[i][2:]
+        src, dst = buf.at[2], buf.at[1]
+        if rows is not None:
+            src, dst = src.at[rows], dst.at[rows]
+        return pltpu.make_async_remote_copy(
+            src_ref=src, dst_ref=dst, send_sem=fsend.at[i], recv_sem=hrecv.at[1, i], device_id=along_x(3)
+        )
 
     lane = lax.broadcasted_iota(jnp.int32, (1, 128), 1)
     row8 = lax.broadcasted_iota(jnp.int32, (8, tok), 0)
@@ -190,9 +201,23 @@
     early()
     for i in range(len(pieces)):
         pass_on(i)
+    for i in range(len(pieces)):
+
+        @pl.when(handing)
+        def _(i=i):
+            along(i, 3, False).wait_recv()
+            hand_on(i).start()
+
     for d in range(1, REACH + 1):
         for i in range(len(pieces)):
-            along(i, d, False).wait_recv()
+            if d == 3:
+
+                @pl.when(jnp.logical_not(handing))
+                def _(i=i):
+                    along(i, 3, False).wait_recv()
+
+            else:
+                along(i, d, False).wait_recv()
         prepare(mbuf[d - 1], kbuf.at[d - 1], vbuf[d - 1])
         if d < REACH:
 
@@ -250,8 +275,16 @@
             def _(i=i):
                 across(i).wait_send()
 
-            for d in range(1, REACH + 1):
-                along(i, d, False).wait_send()
+            along(i, 1, False).wait_send()
+            along(i, 3, False).wait_send()
+
+            @pl.when(x + 2 < EPG)
+            def _(i=i):
+                along(i, 2, False).wait_send()
+
+            @pl.when(handing)
+            def _(i=i):
+                hand_on(i).wait_send()
 
     return drain
 
@@ -560,7 +593,7 @@
         pltpu.VMEM((span, heads), BF16),
         pltpu.VMEM((n_tp, tok, heads), BF16),
         dma((3,)),
-        dma((1 + 2 * CUTS,)), dma((1 + 2 * CUTS,)),
+        dma((1 + 2 * CUTS,)), dma((1 + 2 * CUTS,)), dma((1 + 2 * CUTS,)),
         dma((REACH, 1 + 2 * CUTS)), dma((REACH, 1 + 2 * CUTS)),
         dma((n_tp,)), dma((n_tp,)),
     ]

time: 141 us -> 139 us (0.986)
  Pallas kernels: 139 us -> 137 us
    pallas_call x1, Pallas kernels: 139 us -> 137 us  [layer(): pl.pallas_call(functools.partial(layer_kernel, n_sp, n_tp, capacity, part...]
where the time goes in v6:
time: 139 us
  Pallas kernels  137 us (99%)
  local copies, waits for them, and re-layouts  1.88 us (1%)
    pallas_call x1, Pallas kernels, layer(): pl.pallas_call(functools.partial(layer_kernel, n_sp, n_tp, capacity, part...  137 us

profile of v6, /device:TPU:2, one launch (start us, length us, event | category | flops | bytes accessed | tf_op | source)
XLA Modules:
  0.0 138.6 jit_solution(12804488353104011475)
XLA Ops:
  0.0 136.7 %layer.1 = bf16[128,2048]{1,0:T(8,128)(2,1)} custom-call(bf16[1024,128]{1,0:T(8,128)(2,1)} %refs_0_.1, bf16[1024,128]{1,0:T(8,128)(2,1)} %refs_1_.1, bf16[1024,128]{1,0:T(8,128)(2,1)} %refs_2_.1, f32[2,1024]{1,0:T(2,128)} %refs_3_.1, s32[1,1024]{1,0:T(1,128)} %bitcast.11, f32[1,2048]{1,0:T(1,128)} %bitcast.10, s32[2,128]{1,0:T(2,128)} %bitcast.12, ...), custom_call_target="tpu_custom_call" | custom-call | tf_op jit(solution)/shard_map/layer/pallas_call | solution.py:620
  136.7 1.9 %copy.15 = bf16[128,2048]{1,0:T(8,128)(2,1)} copy(bf16[128,2048]{1,0:T(8,128)(2,1)} %layer.1) | data formatting | bytes 1048576

commit v7 on v6

--- a/solution.py
+++ b/solution.py
@@ -13,7 +13,7 @@
 QF = 1024
 KT = 512
 FAR = -1e30
-CUTS = 2
+CUTS = 4
 
 norm_eps = 1e-06
 F32 = jnp.float32
@@ -370,9 +370,9 @@
         table = [table, rest, jnp.zeros((16, 64), F32)] if s % 2 == 0 else [jnp.zeros((16, 64), F32), table, rest]
         table = jnp.concatenate(table, axis=1)
         if s == HERE:
-            mbuf[s] = table
+            mbuf[s] = table.astype(BF16)
         else:
-            ms[s] = table
+            ms[s] = table.astype(BF16)
     sel = jnp.concatenate(sel, axis=0).astype(BF16)
     wide = lax.broadcasted_iota(jnp.int32, (tok, tok), 0)
     cols = jnp.transpose(jnp.where(wide == 0, mine, jnp.where(wide == 1, place, 0.0)))
@@ -439,10 +439,10 @@
             s = 2 * p + half
             if s != HERE:
                 mcopy(s).wait_recv()
-            table = jnp.concatenate([mbuf[s], jnp.zeros((112, 128), F32)], axis=0)
+            table = jnp.concatenate([mbuf[s].astype(F32), jnp.zeros((112, 128), F32)], axis=0)
             mcol[s] = jnp.transpose(table)[64 * half : 64 * half + group, :]
-        second = mbuf[2 * p + 1]
-        table = mbuf[2 * p] + jnp.where(second > 0.0, second + float(capacity), 0.0)
+        second = mbuf[2 * p + 1].astype(F32)
+        table = mbuf[2 * p].astype(F32) + jnp.where(second > 0.0, second + float(capacity), 0.0)
         want = lax.broadcasted_iota(jnp.int32, (group, 128), 0).astype(F32) + 1.0
         rows = [jnp.where(table[h : h + 1, :] == want, 1.0, 0.0) for h in range(EPG)]
         order = jnp.concatenate(rows, axis=0).astype(BF16)
@@ -606,8 +606,8 @@
         pltpu.VMEM((tok, width), F32),
         pltpu.VMEM((tok, width), BF16),
         slots, slots,
-        pltpu.VMEM((planes, 16, 128), F32),
-        pltpu.VMEM((planes, 16, 128), F32),
+        pltpu.VMEM((planes, 16, 128), BF16),
+        pltpu.VMEM((planes, 16, 128), BF16),
         pltpu.VMEM((planes, group, 128), F32),
         quads, quads, quads, quads,
         slots, slots,

time: 139 us -> 140 us (level)
  no operation moved by 1% of the time
where the time goes in v7:
time: 140 us
  Pallas kernels  138 us (99%)
  local copies, waits for them, and re-layouts  1.88 us (1%)
    pallas_call x1, Pallas kernels, layer(): pl.pallas_call(functools.partial(layer_kernel, n_sp, n_tp, capacity, part...  138 us

profile of v7, /device:TPU:2, one launch (start us, length us, event | category | flops | bytes accessed | tf_op | source)
XLA Modules:
  0.0 139.6 jit_solution(9333088213885018631)
XLA Ops:
  0.0 137.7 %layer.1 = bf16[128,2048]{1,0:T(8,128)(2,1)} custom-call(bf16[1024,128]{1,0:T(8,128)(2,1)} %refs_0_.1, bf16[1024,128]{1,0:T(8,128)(2,1)} %refs_1_.1, bf16[1024,128]{1,0:T(8,128)(2,1)} %refs_2_.1, f32[2,1024]{1,0:T(2,128)} %refs_3_.1, s32[1,1024]{1,0:T(1,128)} %bitcast.11, f32[1,2048]{1,0:T(1,128)} %bitcast.10, s32[2,128]{1,0:T(2,128)} %bitcast.12, ...), custom_call_target="tpu_custom_call" | custom-call | tf_op jit(solution)/shard_map/layer/pallas_call | solution.py:620
  137.7 1.9 %copy.15 = bf16[128,2048]{1,0:T(8,128)(2,1)} copy(bf16[128,2048]{1,0:T(8,128)(2,1)} %layer.1) | data formatting | bytes 1048576
